TPU v7x, 128 devices: a whole 4x4x4 slice. The times are simulated.
128 devices in a mesh: sp: 32 (over z, y, core), tp: 4 (over x).
Axes of the slice: x: 4, y: 4, z: 4, core: 2. Of those that a mesh axis runs over, the one named last changes fastest.
Arguments:
- hidden: bfloat16 [8192, 4096], P('sp'), as said below
- key_weight: bfloat16 [4096, 1024], P(None, 'tp'), as said below
- queries: bfloat16 [8192, 4096], P('sp', 'tp'), as said below
- values: bfloat16 [8192, 1024], P('sp', 'tp'), as said below
- map_out: bfloat16 [8192, 8192], P('sp', 'tp'), as said below
- log_sums: float32 [32, 8192], P('tp', 'sp'), as said below
- out_grad: bfloat16 [8192, 4096], P('sp', 'tp'), may hold values from -6 to 6
- mixing: float32 [16], P('tp'), may hold values from 0.3 to 0.8
- out_gain: float32 [256], replicated, may hold values from 0.1 to 1.9
Outputs:
- grad_query: bfloat16 [8192, 4096], P('sp', 'tp')
- grad_key: bfloat16 [8192, 1024], P('sp', 'tp')
- grad_value: bfloat16 [8192, 1024], P('sp', 'tp')
- grad_weight: float32 [4096, 1024], P('sp', 'tp')
Inputs may be any that keep to these rules, and one draw needn't show every extreme that they name: `hidden`: inputs of order one. `key_weight`: entries of order 1 / sqrt(4096) times a constant. `queries`: entries of order one. `values`: entries of order one. `map_out`: for head h and map m: the row's weights exp(scores - log_sums) over keys j <= i times the values of key head g(h), rounded to bfloat16.
All inputs are finite; a program needn't handle non-finite values.
Results may differ from a plain program's by a relative error of at most 0.02.
Values may be sent and summed in bfloat16 or wider, within the bound.
A program may use at most 256 MiB of HBM per device.

v0:
```python
import jax
import jax.numpy as jnp
from jax import lax
from jax.sharding import PartitionSpec as P

HEAD_DIM = 128
V_DIM = 256


OUT_SCALE = 0.8
NORM_EPS = 1e-06


def sent_together(arrays, axis, dim, along):
    widths = [a.shape[along] for a in arrays]
    both = jnp.concatenate(arrays, axis=along)
    filled = lax.all_gather(both, axis, axis=dim, tiled=True)
    return tuple(jnp.split(filled, [sum(widths[:k]) for k in range(1, len(widths))], axis=along))


def side_by_side(arrays, axis, dim, along):
    both = jnp.concatenate(arrays, axis=along)
    filled, at, outs = (lax.psum_scatter(both, axis, scatter_dimension=dim, tiled=True), 0, [])
    for a in arrays:
        outs.append(lax.slice_in_dim(filled, at, at + a.shape[along], axis=along))
        at += a.shape[along]
    return tuple(outs)


def in_blocks(value, dim, peers):
    lengths = value.shape
    blocks = value.reshape(*lengths[:dim], peers, lengths[dim] // peers, *lengths[dim + 1 :])
    return jnp.moveaxis(blocks, dim, 0)


def sent_and_summed(value, axis, dim):
    peers = lax.axis_size(axis)
    blocks = lax.all_to_all(in_blocks(value, dim, peers), axis, 0, 0, tiled=True)
    return jnp.sum(blocks.astype(jnp.float32), axis=0)


def head_terms(out_grad, map_out, mixing, out_gain):
    rows_here = out_grad.shape[0]
    heads_here = mixing.shape[0]
    v_width = out_gain.shape[0]
    maps_out = map_out.astype(jnp.float32).reshape(rows_here, heads_here, 2, v_width)
    pre_norm = maps_out[:, :, 0] - mixing[None, :, None] * maps_out[:, :, 1]
    inverse = lax.rsqrt(jnp.mean(pre_norm * pre_norm, axis=-1, keepdims=True) + NORM_EPS)
    upstream = (
        out_grad.astype(jnp.float32).reshape(rows_here, heads_here, v_width) * out_gain * OUT_SCALE
    )
    d_out = inverse * (
        upstream
        - pre_norm * inverse * inverse * jnp.mean(upstream * pre_norm, axis=-1, keepdims=True)
    )
    row_terms = jnp.sum(d_out[:, :, None, :] * maps_out, axis=-1).reshape(rows_here, heads_here * 2)
    return (d_out.reshape(rows_here, heads_here * v_width).astype(jnp.bfloat16), row_terms)


def block_grads(query_blk, d_blk, stats_blk, query_pos, key_part, value_part, key_pos, mix_blk):
    n_rows, n_groups, per_group = (query_blk.shape[0], query_blk.shape[1], query_blk.shape[2])
    scale = query_blk.shape[-1] ** (-0.5)
    stat_cols = 2 * n_groups * per_group
    log_part = jnp.transpose(
        stats_blk[:, :stat_cols].reshape(n_rows, n_groups, per_group, 2), (1, 2, 3, 0)
    )[..., None]
    term_part = jnp.transpose(
        stats_blk[:, stat_cols:].reshape(n_rows, n_groups, per_group, 2), (1, 2, 3, 0)
    )[..., None]
    scores = (
        jnp.einsum("rgpmd,kgmd->gpmrk", query_blk, key_part, preferred_element_type=jnp.float32)
        * scale
    )
    visible = key_pos[None, :] <= query_pos[:, None]
    probs_map = jnp.exp(jnp.where(visible, scores - log_part, -1e30))
    d_attn = jnp.einsum("rgpv,kgv->gprk", d_blk, value_part, preferred_element_type=jnp.float32)
    mix_cols = mix_blk[:, :, None, None]
    weights_a = (probs_map[:, :, 0] - mix_cols * probs_map[:, :, 1]).astype(jnp.bfloat16)
    d_scores = jnp.stack(
        [
            probs_map[:, :, 0] * (d_attn - term_part[:, :, 0]),
            -mix_cols * probs_map[:, :, 1] * (d_attn - term_part[:, :, 1]),
        ],
        axis=2,
    ).astype(jnp.bfloat16)
    grad_q = (
        jnp.einsum("gpmrk,kgmd->rgpmd", d_scores, key_part, preferred_element_type=jnp.float32)
        * scale
    )
    grad_k = (
        jnp.einsum("gpmrk,rgpmd->kgmd", d_scores, query_blk, preferred_element_type=jnp.float32)
        * scale
    )
    grad_v = jnp.einsum("gprk,rgpv->kgv", weights_a, d_blk, preferred_element_type=jnp.float32)
    return (grad_q, grad_k, grad_v)


def on_device(hidden, key_weight, queries, values, map_out, log_sums, out_grad, mixing, out_gain):
    n_rows = queries.shape[0]
    heads_here = mixing.shape[0]
    groups_here = values.shape[1] // V_DIM
    per_group = heads_here // groups_here
    sp_count = lax.axis_size("sp")
    sp_index = lax.axis_index("sp")
    total = n_rows * sp_count
    key_rows = jnp.dot(hidden, key_weight, preferred_element_type=jnp.float32).astype(jnp.bfloat16)
    d_rows, row_terms = head_terms(out_grad, map_out, mixing, out_gain)
    stats = jnp.concatenate([log_sums.T, row_terms], axis=1)
    positions = sp_index * n_rows + jnp.arange(n_rows, dtype=jnp.int32)
    mix_blk = mixing.reshape(groups_here, per_group)
    k_cols = key_rows.shape[1]
    v_cols = values.shape[1]
    q_cols = queries.shape[1]
    query_blk = queries.reshape(n_rows, groups_here, per_group, 2, HEAD_DIM)
    d_blk = d_rows.reshape(n_rows, groups_here, per_group, V_DIM)

    def block_terms(key_piece, value_piece):
        n_keys = key_piece.shape[0]
        key_pos = jnp.arange(n_keys, dtype=jnp.int32)
        grad_q, grad_k, grad_v = block_grads(
            query_blk,
            d_blk,
            stats,
            positions,
            key_piece.reshape(n_keys, groups_here, 2, HEAD_DIM),
            value_piece.reshape(n_keys, groups_here, V_DIM),
            key_pos,
            mix_blk,
        )
        return (
            grad_q.reshape(n_rows, q_cols),
            grad_k.reshape(n_keys, k_cols),
            grad_v.reshape(n_keys, v_cols),
        )

    grad_acc = jnp.zeros((n_rows, q_cols), jnp.float32)
    key_full = jnp.zeros((total, k_cols), jnp.float32)
    value_full = jnp.zeros((total, v_cols), jnp.float32)
    key_piece, value_piece = sent_together((key_rows, values), "sp", 0, 1)
    n_keys = key_piece.shape[0]

    def active(state):
        grad_q, grad_k, grad_v = block_terms(key_piece, value_piece)
        return (grad_q, grad_k, grad_v)

    def passive(state):
        return state

    grad_acc, key_full, value_full = lax.cond(
        jnp.int32(0) <= positions[-1], active, passive, (grad_acc, key_full, value_full)
    )
    key_own, value_own = tuple(
        (
            part.astype(jnp.float32)
            for part in side_by_side(
                (key_full.astype(jnp.bfloat16), value_full.astype(jnp.bfloat16)), "sp", 0, 1
            )
        )
    )
    grad_key = key_own.astype(jnp.bfloat16)
    grad_value = value_own.astype(jnp.bfloat16)
    grad_query = grad_acc.astype(jnp.bfloat16)
    grad_weight = sent_and_summed(
        lax.dot_general(
            hidden, grad_key, (((0,), (0,)), ((), ())), preferred_element_type=jnp.float32
        ).astype(jnp.bfloat16),
        "sp",
        0,
    )
    return (grad_query, grad_key, grad_value, grad_weight)


def solution(mesh):
    placed = (
        P("sp", None),
        P(None, "tp"),
        P("sp", "tp"),
        P("sp", "tp"),
        P("sp", "tp"),
        P("tp", "sp"),
        P("sp", "tp"),
        P("tp"),
        P(),
    )
    return jax.shard_map(
        on_device,
        mesh=mesh,
        in_specs=placed,
        out_specs=(P("sp", "tp"), P("sp", "tp"), P("sp", "tp"), P("sp", "tp")),
        check_vma=False,
    )
```

profile of v0, /device:TPU:1, one launch (start us, length us, event | category | flops | bytes accessed | tf_op | source)
XLA Modules:
  0.0 379.9 jit_solution(1946363696503191250)
XLA Ops:
  7.2 0.0 copy-start
  7.2 0.0 copy-start.2
  7.2 0.0 all-gather.2.cloned.1.call-start
  7.2 1.2 copy.84
  8.4 0.4 copy-done
  8.8 0.0 copy-start.5
  8.8 2.5 convolution_convert_fusion.1
  11.4 0.7 pad_maximum_fusion.16
  12.1 0.0 all-gather.2.cloned.1.call-update
  12.1 0.0 reduce-scatter.2.cloned.1.call-start
  12.2 2.5 reshape.193
  14.7 2.1 convert_element_type.89
  16.8 0.0 copy-done.2
  16.8 3.1 reshape.197
  19.9 9.9 %slice_reduce_fusion = (f32[256,4,256]{2,1,0:T(4,128)S(1)}, f32[256,4,256]{2,1,0:T(4,128)S(1)}, f32[256,4,1,256]{3,2,1,0:T(1,128)S(1)}, f32[256,4,1,256]{3,2,1,0:T(1,128)S(1)}) fusion(f32[256,4,2,256]{3,2,1,0:T(2,128)} %reshape.197), kind=kLoop, calls=%fused_computation.67 | loop fusion | bytes 6291456 | tf_op jit(solution)/shard_map/slice | solution.py:47
  29.8 0.0 copy-start.1
  29.8 1.0 copy-done.1
  30.8 0.0 copy-done.5
  30.8 0.0 copy-done.7
  30.8 2.3 multiply_reduce_fusion.1
  33.1 0.0 copy-start.6
  33.1 0.3 mul.230
  33.4 1.2 copy.107
  34.6 0.3 mul.249
  34.9 1.2 copy.112
  36.1 1.2 copy.109
  37.4 1.2 copy.111
  38.5 0.1 broadcast_bitcast_fusion
  38.6 0.6 slice.33
  39.9 3.7 fusion.43
  43.5 31.3 %all-gather.2.cloned.1.call-done = bf16[8192,512]{0,1:T(8,128)(2,1)} async-done(((bf16[256,512]{0,1:T(8,128)(2,1)}), bf16[8192,512]{0,1:T(8,128)(2,1)}) %all-gather.2.cloned.1.call-update) | async-done | bytes 8388624 | tf_op jit(solution)/shard_map/all_gather | solution.py:17
  74.8 0.0 copy-done.6
  74.8 154.6 %conditional.1 = (bf16[8192,256]{0,1:T(8,128)(2,1)}, bf16[8192,256]{1,0:T(8,128)(2,1)}, bf16[256,1024]{1,0:T(8,128)(2,1)}) conditional(s32[]{:T(128)} %bitcast.37, () %tuple.24, (s32[256]{0:T(256)S(1)}, bf16[8192,512]{0,1:T(8,128)(2,1)}, bf16[256,1024]{1,0:T(8,128)(2,1)}, f32[256,8]{0,1:T(8,128)S(1)}, bf16[256,1024]{1,0:T(8,128)(2,1)}, ...), branch_computations={%region_2.0_spmd, %region_3.5_spmd} | conditional | flops 21705259008 | bytes 370772128 | solution.py:149
  74.8 4.6 %split.8 = bf16[8192,256]{0,1:T(8,128)(2,1)} slice(bf16[8192,512]{0,1:T(8,128)(2,1)} %get-tuple-element.181), slice={[0:8192], [0:256]} | slice | bytes 8388608 | tf_op jit(solution)/shard_map/split | solution.py:18
  79.4 2.2 reshape.183
  81.6 2.0 copy.82
  83.6 2.7 iota_compare_fusion
  86.3 29.1 %fusion.1 = f32[1,4,2,256,8192]{3,4,1,2,0:T(8,128)} fusion(f32[4,2,256]{2,0,1:T(4,128)S(1)} %bitcast.187, pred[256,8192]{0,1:T(8,128)(4,1)} %iota_compare_fusion, bf16[8192,2,128,1]{0,2,3,1:T(8,128)(2,1)} %bitcast.175, bf16[256,4,2,128]{0,3,1,2:T(8,128)(2,1)} %copy.82), kind=kOutput, calls=%fused_computation.2 | convolution fusion | flops 4345298944 | bytes 73932800 | tf_op jit(solution)/shard_map/cond/branch_1_fun/rgpmd,kgmd->gpmrk/dot_general | solution.py:71
  115.4 2.7 reshape.186
  118.1 2.5 fusion.32
  120.5 3.1 multiply_reduce_fusion
  123.6 0.3 fusion.45
  123.9 0.2 copy.77
  124.1 0.2 copy.78
  124.4 0.0 copy-start.3
  124.4 12.0 %copy.85 = bf16[8192,512]{1,0:T(8,128)(2,1)} copy(bf16[8192,512]{0,1:T(8,128)(2,1)} %get-tuple-element.181) | data formatting | bytes 16777216 | tf_op jit(solution)/shard_map
  136.4 0.0 copy-done.3
  136.4 34.2 %fusion.11 = (bf16[4,1,256,8192]{2,3,0,1:T(8,128)(2,1)}, bf16[4,1,256,8192]{2,3,0,1:T(8,128)(2,1)}) fusion(f32[1,4,2,256,8192]{3,4,1,2,0:T(8,128)} %fusion.1, f32[4,256]{1,0:T(4,128)S(1)} %bitcast.188, f32[4,256]{1,0:T(4,128)S(1)} %bitcast.189, f32[4]{0:T(128)S(1)} %neg.4, bf16[32,4,8,256]{3,2,1,0:T(8,128)(2,1)S(1)} %bitcast.182, bf16[8192,512]{1,0:T(8,128)(2,1)} %copy.85), kind=kOutput, calls=%fused_computation.17 | convolution fusion | flops 4353687552 | bytes 105390096 | tf_op jit(solution)/shard_map/cond/branch_1_fun/rgpv,kgv->gprk/dot_general | solution.py:76
  170.5 14.9 %fusion.26 = bf16[256,1,4,2,128]{0,4,2,3,1:T(8,128)(2,1)} fusion(bf16[8192,2,128,1]{0,2,3,1:T(8,128)(2,1)} %bitcast.176, bf16[4,1,256,8192]{2,3,0,1:T(8,128)(2,1)} %get-tuple-element.203, bf16[4,1,256,8192]{2,3,0,1:T(8,128)(2,1)} %get-tuple-element.202), kind=kOutput, calls=%fused_computation.30 | convolution fusion | flops 4362600448 | bytes 38273024 | tf_op jit(solution)/shard_map/cond/branch_1_fun/gpmrk,kgmd->rgpmd/dot_general | solution.py:87
  185.4 1.1 copy.80
  186.5 1.0 copy.101
  187.5 17.8 %fusion.19 = bf16[2,8192,128]{1,2,0:T(8,128)(2,1)} fusion(bf16[256,4,2,128]{0,3,1,2:T(8,128)(2,1)} %copy.82, bf16[4,1,256,8192]{2,3,0,1:T(8,128)(2,1)} %get-tuple-element.203, bf16[4,1,256,8192]{2,3,0,1:T(8,128)(2,1)} %get-tuple-element.202), kind=kOutput, calls=%fused_computation.22 | convolution fusion | flops 4315938816 | bytes 38273024 | tf_op jit(solution)/shard_map/cond/branch_1_fun/gpmrk,rgpmd->kgmd/dot_general | solution.py:91
  205.3 24.1 %fusion.20 = bf16[8192,256]{1,0:T(8,128)(2,1)} fusion(f32[1,4,2,256,8192]{3,4,1,2,0:T(8,128)} %fusion.1, f32[4]{0:T(128)S(1)} %get-tuple-element.105, bf16[32,4,8,256]{3,2,1,0:T(8,128)(2,1)S(1)} %bitcast.183), kind=kOutput, calls=%fused_computation.23 | convolution fusion | flops 4322230272 | bytes 71827472 | tf_op jit(solution)/shard_map/cond/branch_1_fun/gprk,rgpv->kgv/dot_general | solution.py:94
  229.4 6.4 %copy.88 = bf16[8192,256]{1,0:T(8,128)(2,1)} copy(bf16[8192,256]{0,1:T(8,128)(2,1)} %get-tuple-element.117) | data formatting | bytes 8388608 | tf_op jit(solution)/shard_map/cond | solution.py:149
  235.8 7.3 %pad_maximum_fusion.15 = bf16[8192,512]{1,0:T(8,128)(2,1)} fusion(bf16[8192,256]{1,0:T(8,128)(2,1)} %get-tuple-element.118, bf16[8192,256]{1,0:T(8,128)(2,1)} %copy.88), kind=kLoop, calls=%fused_computation.46 | loop fusion | flops 16777216 | bytes 16777216 | tf_op jit(solution)/shard_map/concatenate | solution.py:22
  243.0 0.0 reduce-scatter.2.cloned.1.call-update
  243.1 90.5 %reduce-scatter.2.cloned.1.call-done = bf16[256,512]{1,0:T(8,128)(2,1)} async-done(((bf16[8192,512]{1,0:T(8,128)(2,1)}), bf16[256,512]{1,0:T(8,128)(2,1)}) %reduce-scatter.2.cloned.1.call-update) | async-done | bytes 262160 | tf_op jit(solution)/shard_map/reduce_scatter | solution.py:23
  333.6 1.6 fusion.46
  335.2 0.7 fusion.39
  336.0 0.6 copy.153
  336.6 35.4 %all_to_all.5 = bf16[32,128,256]{1,2,0:T(8,128)(2,1)S(1)} all-to-all(bf16[32,128,256]{1,2,0:T(8,128)(2,1)S(1)} %bitcast.169), channel_id=1, replica_groups=mesh['sp'=32,'tp'=4] {'sp'}, dimensions={0} | all-to-all | bytes 4194304 | tf_op jit(solution)/shard_map/all_to_all | solution.py:38
  372.0 0.3 convert_reduce_fusion
  372.3 0.8 copy.92
  373.0 0.0 copy-done.4
  (10 shorter events, 0.1 us)
Async XLA Ops:
  7.2 1.7 copy-start
  7.2 9.6 %copy-start.2 = (bf16[256,2048]{1,0:T(8,128)(2,1)S(1)}, bf16[256,2048]{1,0:T(8,128)(2,1)}, u32[]{:S(2)}) copy-start(bf16[256,2048]{1,0:T(8,128)(2,1)} %param.15) | copy-start | bytes 3145732
  7.2 67.6 %all-gather.2.cloned.1.call-start = ((), (), s32[]{:S(2)}) async-start(), calls=%async_computation.2 | async-start | bytes 8650752 | tf_op jit(solution)/shard_map/all_gather | solution.py:17
  8.8 22.0 %copy-start.5 = (f32[256]{0:T(256)S(1)}, f32[256]{0:T(256)}, u32[]{:S(2)}) copy-start(f32[256]{0:T(256)} %param.19) | copy-start | bytes 3076
  8.8 22.0 %copy-start.7 = (f32[4]{0:T(128)S(1)}, f32[4]{0:T(128)}, u32[]{:S(2)}) copy-start(f32[4]{0:T(128)} %param.18) | copy-start | bytes 52
  12.1 321.5 %reduce-scatter.2.cloned.1.call-start = ((), (), s32[]{:S(2)}) async-start(), calls=%async_computation.3 | async-start | bytes 8650752 | tf_op jit(solution)/shard_map/reduce_scatter | solution.py:23
  29.8 1.0 copy-start.1
  33.1 41.8 %copy-start.6 = (f32[8,256]{1,0:T(8,128)S(1)}, f32[8,256]{1,0:T(8,128)}, u32[]{:S(2)}) copy-start(f32[8,256]{1,0:T(8,128)} %param.16) | copy-start | bytes 24580
  124.4 12.0 %copy-start.3 = (bf16[256,1024]{1,0:T(8,128)(2,1)S(1)}, bf16[256,1024]{1,0:T(8,128)(2,1)}, u32[]{:S(2)}) copy-start(bf16[256,1024]{1,0:T(8,128)(2,1)} %get-tuple-element.100) | copy-start | bytes 1572868 | tf_op jit(solution)/shard_map/cond
  335.2 37.8 %copy-start.4 = (bf16[256,256]{1,0:T(8,128)(2,1)}, bf16[256,256]{1,0:T(8,128)(2,1)S(1)}, u32[]{:S(2)}) copy-start(bf16[256,256]{1,0:T(8,128)(2,1)S(1)} %get-tuple-element.209) | copy-start | bytes 393220
Sparse Core Ops, SparseCore 0:
  12.2 62.5 all-gather.1
  243.2 90.3 reduce-scatter.1
where the time goes:
time: 381 us; the launch traced here: 380 us
  matrix products  123 us (32%)
  waiting for transfers between devices  122 us (32%)
  local copies, waits for them, and re-layouts  59.7 us (16%)
  blocking collectives  35.4 us (9%)
  other arithmetic  24.7 us (6%)
  between operations  14.8 us (4%)
    reduce_scatter x1, waiting for transfers between devices, side_by_side(): lax.psum_scatter(both, axis, scatter_dimension=dim, tiled=True)  90.5 us
    all_to_all x1, blocking collectives, sent_and_summed(): lax.all_to_all(in_blocks(value, dim, peers), axis, 0, 0, tiled=True)  35.4 us
    dot_general x1, matrix products, block_grads(): jnp.einsum('rgpv,kgv->gprk', d_blk, value_part, preferred_element_type=jn...  34.2 us
    all_gather x1, waiting for transfers between devices, sent_together(): filled = lax.all_gather(both, axis, axis=dim, tiled=True)  31.3 us
    dot_general x1, matrix products, block_grads(): jnp.einsum('rgpmd,kgmd->gpmrk', query_blk, key_part, preferred_element_ty...  29.1 us
    dot_general x1, matrix products, block_grads(): jnp.einsum('gprk,rgpv->kgv', weights_a, d_blk, preferred_element_type=jnp...  24.1 us
    dot_general x1, matrix products, block_grads(): jnp.einsum('gpmrk,rgpmd->kgmd', d_scores, query_blk, preferred_element_ty...  17.8 us
    another operation x3, local copies, waits for them, and re-layouts  16.2 us
  transfers between devices with their start and end apart: 2, of which 2 were waited for; matrix products, arithmetic and copies ran while one was open for 8% of the time, Pallas kernels for 0%

commit v1 on v0

v1 whole, which is shorter than its diff:
```python
import functools
import math

import jax
import jax.numpy as jnp
from jax import lax
from jax.experimental import pallas as pl
from jax.experimental.pallas import tpu as pltpu
from jax.sharding import PartitionSpec as P

HEAD_DIM = 128
V_DIM = 256
OUT_SCALE = 0.8
NORM_EPS = 1e-06
LOG2E = math.log2(math.e)
MESH_ID = pl.DeviceIdType.MESH
BF16 = jnp.bfloat16
F32 = jnp.float32


def nn(a, b):
    return jnp.dot(a, b, preferred_element_type=F32)


def kernel(n, heads, mix_ref, hid_hbm, kw_hbm, q_hbm, val_hbm, map_hbm, log_hbm, og_hbm, gain_hbm,
           gq_ref, gk_ref, gv_ref, gw_ref,
           hid, kw, maps, logs, og, gain, kbuf, vbuf, kt, qn, dn, qt, dt, stats, dqt, dq_got,
           ds_a, ds_b, w_a, own_k, own_v, term_out, term_in, dw_out, dw_in,
           ld, k_send, k_recv, v_send, v_recv, t_send, t_recv, w_send, w_recv, x_send, x_recv):
    chips = n // 2
    me = lax.axis_index("sp")
    tp = lax.axis_index("tp")
    u = me // 2
    c = me % 2
    rows = hid.shape[0]
    scale = HEAD_DIM ** (-0.5)
    partner = 2 * u + 1 - c
    width = hid.shape[1] // n

    barrier = pltpu.get_barrier_semaphore()

    def greet(i, carry):
        peer = lax.rem(me + i, n)
        pl.semaphore_signal(barrier, inc=1, device_id=(peer, tp), device_id_type=MESH_ID)
        return carry

    lax.fori_loop(1, n, greet, 0)

    my_rows = pl.ds(pl.multiple_of(c * rows, rows), rows)
    its_rows = pl.ds(pl.multiple_of((1 - c) * rows, rows), rows)
    loads = [
        pltpu.make_async_copy(kw_hbm, kw, ld.at[0]),
        pltpu.make_async_copy(hid_hbm, hid, ld.at[1]),
        pltpu.make_async_copy(val_hbm, vbuf.at[u], ld.at[2]),
        pltpu.make_async_copy(map_hbm, maps, ld.at[3]),
        pltpu.make_async_copy(og_hbm, og, ld.at[4]),
        pltpu.make_async_copy(gain_hbm, gain, ld.at[5]),
        pltpu.make_async_copy(log_hbm, logs, ld.at[6]),
        pltpu.make_async_copy(q_hbm, qn.at[my_rows, :], ld.at[7]),
    ]
    for load in (loads[2], loads[0], loads[1], loads[7], loads[3], loads[4], loads[5], loads[6]):
        load.start()

    def to(src, dst, s_sem, r_sem, device):
        return pltpu.make_async_remote_copy(
            src_ref=src, dst_ref=dst, send_sem=s_sem, recv_sem=r_sem,
            device_id=(device, tp), device_id_type=MESH_ID)

    def k_copy(slot, dest):
        return to(kbuf.at[slot], kbuf.at[slot], k_send.at[dest], k_recv.at[slot], 2 * dest + c)

    def v_copy(slot, dest):
        return to(vbuf.at[slot], vbuf.at[slot], v_send.at[dest], v_recv.at[slot], 2 * dest + c)

    def t_copy(dest, source):
        return to(term_out.at[dest], term_in.at[source], t_send.at[dest], t_recv.at[source], 2 * dest + c)

    def w_copy(dest, source):
        return to(dw_out.at[dest], dw_in.at[source], w_send.at[dest], w_recv.at[source], dest)

    loads[2].wait()
    loads[7].wait()
    pl.semaphore_wait(barrier, n - 1)

    q_swap = to(qn.at[my_rows, :], qn.at[my_rows, :], x_send.at[0], x_recv.at[0], partner)
    q_swap.start()

    def send_v(i, carry):
        v_copy(u, chips - 1 - i).start()
        return carry

    lax.fori_loop(0, chips - 1 - u, send_v, 0)

    loads[0].wait()
    loads[1].wait()
    kbuf[u] = nn(hid[...], kw[...]).astype(BF16)

    for load in loads[3:7]:
        load.wait()

    def send_k(i, carry):
        k_copy(u, chips - 1 - i).start()
        return carry

    lax.fori_loop(0, chips - 1 - u, send_k, 0)

    lane = lax.broadcasted_iota(jnp.int32, (rows, 128), 1)
    terms = jnp.zeros((rows, 128), F32)
    for h in range(heads):
        mix = mix_ref[h]
        first = maps[:, (2 * h) * V_DIM:(2 * h + 1) * V_DIM].astype(F32)
        second = maps[:, (2 * h + 1) * V_DIM:(2 * h + 2) * V_DIM].astype(F32)
        pre = first - mix * second
        inverse = lax.rsqrt(jnp.mean(pre * pre, axis=-1, keepdims=True) + NORM_EPS)
        up = og[:, h * V_DIM:(h + 1) * V_DIM].astype(F32) * gain[...] * OUT_SCALE
        d_out = inverse * (up - pre * (inverse * inverse * jnp.mean(up * pre, axis=-1, keepdims=True)))
        dn[my_rows, h * V_DIM:(h + 1) * V_DIM] = d_out.astype(BF16)
        terms = jnp.where(lane == 2 * h, jnp.sum(d_out * first, axis=-1, keepdims=True), terms)
        terms = jnp.where(lane == 2 * h + 1, jnp.sum(d_out * second, axis=-1, keepdims=True), terms)
    stats[c, 2 * heads:4 * heads] = terms.T[:2 * heads]
    mix_row = lax.broadcasted_iota(jnp.int32, (2 * heads, rows), 0)
    log_rows = logs[...] * LOG2E
    for h in range(heads):
        shift = jnp.log(jnp.full((2 * heads, rows), mix_ref[h], F32)) * LOG2E
        log_rows = jnp.where(mix_row == 2 * h + 1, log_rows - shift, log_rows)
    stats[c, :2 * heads] = log_rows

    d_swap = to(dn.at[my_rows, :], dn.at[my_rows, :], x_send.at[1], x_recv.at[1], partner)
    s_swap = to(stats.at[c], stats.at[c], x_send.at[2], x_recv.at[2], partner)
    d_swap.start()
    s_swap.start()
    dqt[...] = jnp.zeros_like(dqt)
    q_swap.wait_recv()
    for h in range(2 * heads):
        qt[h * HEAD_DIM:(h + 1) * HEAD_DIM, :] = qn[:, h * HEAD_DIM:(h + 1) * HEAD_DIM].T
    d_swap.wait_recv()
    s_swap.wait_recv()
    for h in range(heads):
        dt[h * V_DIM:(h + 1) * V_DIM, :] = dn[:, h * V_DIM:(h + 1) * V_DIM].T

    q_rows = 2 * rows

    def block(j, masked):
        kk = kbuf[j]
        kt[...] = kk.T
        vv = vbuf[j]
        both = lambda r: jnp.concatenate([stats[0, r:r + 1, :], stats[1, r:r + 1, :]], axis=1)

        def products(h):
            s_a = nn(kk[:, :HEAD_DIM], qt[(2 * h) * HEAD_DIM:(2 * h + 1) * HEAD_DIM, :])
            s_b = nn(kk[:, HEAD_DIM:], qt[(2 * h + 1) * HEAD_DIM:(2 * h + 2) * HEAD_DIM, :])
            d_p = nn(vv, dt[h * V_DIM:(h + 1) * V_DIM, :])
            return s_a, s_b, d_p

        ready = products(0)
        for h in range(heads):
            s_a, s_b, d_p = ready
            if h + 1 < heads:
                ready = products(h + 1)
            x_a = s_a * (scale * LOG2E) - both(2 * h)
            x_b = s_b * (scale * LOG2E) - both(2 * h + 1)
            if masked:
                key_at = c * rows + lax.broadcasted_iota(jnp.int32, (rows, q_rows), 0)
                query_at = lax.broadcasted_iota(jnp.int32, (rows, q_rows), 1)
                seen = key_at <= query_at
                x_a = jnp.where(seen, x_a, -1e30)
                x_b = jnp.where(seen, x_b, -1e30)
            p_a = jnp.exp2(x_a)
            p_b = jnp.exp2(x_b)
            cols = slice(h * q_rows, (h + 1) * q_rows)
            w_h = (p_a - p_b).astype(BF16)
            a_h = (p_a * (d_p - both(2 * heads + 2 * h))).astype(BF16)
            b_h = (p_b * (both(2 * heads + 2 * h + 1) - d_p)).astype(BF16)
            w_a[:, cols] = w_h
            ds_a[:, cols] = a_h
            ds_b[:, cols] = b_h
            dqt[(2 * h) * HEAD_DIM:(2 * h + 1) * HEAD_DIM, :] += nn(kt[:HEAD_DIM, :], a_h)
            dqt[(2 * h + 1) * HEAD_DIM:(2 * h + 2) * HEAD_DIM, :] += nn(kt[HEAD_DIM:, :], b_h)
        g_v = jnp.zeros((rows, V_DIM), F32)
        g_a = jnp.zeros((rows, HEAD_DIM), F32)
        g_b = jnp.zeros((rows, HEAD_DIM), F32)
        for h in range(heads):
            cols = slice(h * q_rows, (h + 1) * q_rows)
            g_a += nn(ds_a[:, cols], qn[:, (2 * h) * HEAD_DIM:(2 * h + 1) * HEAD_DIM])
            g_b += nn(ds_b[:, cols], qn[:, (2 * h + 1) * HEAD_DIM:(2 * h + 2) * HEAD_DIM])
            g_v += nn(w_a[:, cols], dn[:, h * V_DIM:(h + 1) * V_DIM])
        return g_a * scale, g_b * scale, g_v

    def step(j, carry):
        k_copy(j, u).wait_recv()
        v_copy(j, u).wait_recv()
        g_a, g_b, g_v = block(j, False)
        term_out[j, :, :HEAD_DIM] = g_a.astype(BF16)
        term_out[j, :, HEAD_DIM:2 * HEAD_DIM] = g_b.astype(BF16)
        term_out[j, :, 2 * HEAD_DIM:] = g_v.astype(BF16)
        t_copy(j, u).start()
        return carry

    lax.fori_loop(0, u, step, 0)
    g_a, g_b, g_v = block(u, True)
    own_k[:, :HEAD_DIM] = g_a
    own_k[:, HEAD_DIM:] = g_b
    own_v[...] = g_v

    dq_swap = to(dqt.at[:, its_rows], dq_got, x_send.at[3], x_recv.at[3], partner)
    dq_swap.start()

    def gather_terms(i, carry):
        t_copy(u, i).wait_recv()
        own_k[...] += term_in[i, :, :2 * HEAD_DIM].astype(F32)
        own_v[...] += term_in[i, :, 2 * HEAD_DIM:].astype(F32)
        return carry

    lax.fori_loop(u + 1, chips, gather_terms, 0)
    gk_ref[...] = own_k[...].astype(BF16)
    gv_ref[...] = own_v[...].astype(BF16)
    kt[...] = own_k[...].T.astype(BF16)

    def project(i, carry):
        chip = lax.rem(u + 1 + i, chips)
        piece = nn(kt[...], hid[:, pl.ds(pl.multiple_of(2 * width * chip, 2 * width), 2 * width)]).astype(BF16)
        dw_out[2 * chip] = piece[:, :width]
        dw_out[2 * chip + 1] = piece[:, width:]

        @pl.when(chip != u)
        def _():
            w_copy(2 * chip, me).start()
            w_copy(2 * chip + 1, me).start()

        return carry

    lax.fori_loop(0, chips, project, 0)
    w_copy(partner, me).start()

    dq_swap.wait_recv()
    for h in range(2 * heads):
        part = dqt[h * HEAD_DIM:(h + 1) * HEAD_DIM, my_rows] + dq_got[h * HEAD_DIM:(h + 1) * HEAD_DIM, :]
        gq_ref[:, h * HEAD_DIM:(h + 1) * HEAD_DIM] = (part * scale).T.astype(BF16)

    def add_piece(i, total):
        w_copy(me, i).wait_recv()
        return total + dw_in[i].astype(F32)

    total = dw_out[me].astype(F32)
    total = lax.fori_loop(0, me, add_piece, total)
    total = lax.fori_loop(me + 1, n, add_piece, total)
    gw_ref[...] = total.T

    def v_sent(i, carry):
        v_copy(u, chips - 1 - i).wait_send()
        k_copy(u, chips - 1 - i).wait_send()
        return carry

    lax.fori_loop(0, chips - 1 - u, v_sent, 0)

    def t_sent(j, carry):
        t_copy(j, u).wait_send()
        return carry

    lax.fori_loop(0, u, t_sent, 0)

    def w_sent(i, carry):
        w_copy(lax.rem(me + i, n), me).wait_send()
        return carry

    lax.fori_loop(1, n, w_sent, 0)
    for swap in (q_swap, d_swap, s_swap, dq_swap):
        swap.wait_send()


def on_device(n, hidden, key_weight, queries, values, map_out, log_sums, out_grad, mixing, out_gain):
    rows, model = hidden.shape
    heads = mixing.shape[0]
    k_cols = key_weight.shape[1]
    q_cols = queries.shape[1]
    chips = n // 2
    width = model // n
    vm = pltpu.VMEM
    dma = pltpu.SemaphoreType.DMA
    anywhere = pl.BlockSpec(memory_space=pl.ANY)
    inside = pl.BlockSpec(memory_space=pltpu.VMEM)
    return pl.pallas_call(
        functools.partial(kernel, n, heads),
        out_shape=(
            jax.ShapeDtypeStruct((rows, q_cols), BF16),
            jax.ShapeDtypeStruct((rows, k_cols), BF16),
            jax.ShapeDtypeStruct((rows, V_DIM), BF16),
            jax.ShapeDtypeStruct((width, k_cols), F32),
        ),
        in_specs=[pl.BlockSpec(memory_space=pltpu.SMEM)] + [anywhere] * 8,
        out_specs=(inside,) * 4,
        scratch_shapes=[
            vm((rows, model), BF16),
            vm((model, k_cols), BF16),
            vm((rows, 2 * heads * V_DIM), BF16),
            vm((2 * heads, rows), F32),
            vm((rows, heads * V_DIM), BF16),
            vm((1, V_DIM), F32),
            vm((chips, rows, k_cols), BF16),
            vm((chips, rows, V_DIM), BF16),
            vm((k_cols, rows), BF16),
            vm((2 * rows, q_cols), BF16),
            vm((2 * rows, heads * V_DIM), BF16),
            vm((q_cols, 2 * rows), BF16),
            vm((heads * V_DIM, 2 * rows), BF16),
            vm((2, 4 * heads, rows), F32),
            vm((q_cols, 2 * rows), F32),
            vm((q_cols, rows), F32),
            vm((rows, heads * 2 * rows), BF16),
            vm((rows, heads * 2 * rows), BF16),
            vm((rows, heads * 2 * rows), BF16),
            vm((rows, k_cols), F32),
            vm((rows, V_DIM), F32),
            vm((chips, rows, k_cols + V_DIM), BF16),
            vm((chips, rows, k_cols + V_DIM), BF16),
            vm((n, k_cols, width), BF16),
            vm((n, k_cols, width), BF16),
            dma((8,)),
            dma((chips,)),
            dma((chips,)),
            dma((chips,)),
            dma((chips,)),
            dma((chips,)),
            dma((chips,)),
            dma((n,)),
            dma((n,)),
            dma((4,)),
            dma((4,)),
        ],
        compiler_params=pltpu.CompilerParams(
            collective_id=0, has_side_effects=True, vmem_limit_bytes=62 * 1024 * 1024),
    )(mixing, hidden, key_weight, queries, values, map_out, log_sums, out_grad, out_gain.reshape(1, -1))


def solution(mesh):
    placed = (
        P("sp", None),
        P(None, "tp"),
        P("sp", "tp"),
        P("sp", "tp"),
        P("sp", "tp"),
        P("tp", "sp"),
        P("sp", "tp"),
        P("tp"),
        P(),
    )
    return jax.shard_map(
        functools.partial(on_device, mesh.shape["sp"]),
        mesh=mesh,
        in_specs=placed,
        out_specs=(P("sp", "tp"), P("sp", "tp"), P("sp", "tp"), P("sp", "tp")),
        check_vma=False,
    )
```

time: 381 us -> 164 us (0.43)
  the two profiles are of different devices: /device:TPU:1 before, /device:TPU:81 now
where the time goes in v1:
time: 164 us
  Pallas kernels  157 us (96%)
  local copies, waits for them, and re-layouts  6.57 us (4%)
    pallas_call x1, Pallas kernels, on_device(): pl.pallas_call(functools.partial(kernel, n, heads), out_shape=(jax.ShapeD...  157 us
    unnamed x4, local copies, waits for them, and re-layouts  6.57 us

profile of v1, /device:TPU:81, one launch (start us, length us, event | category | flops | bytes accessed | tf_op | source)
XLA Modules:
  0.0 164.2 jit_solution(10786230022702595880)
XLA Ops:
  0.6 157.0 %shard_map.120 = (bf16[256,1024]{1,0:T(8,128)(2,1)}, bf16[256,256]{1,0:T(8,128)(2,1)}, bf16[256,256]{1,0:T(8,128)(2,1)}, f32[128,256]{1,0:T(8,128)}) custom-call(f32[4]{0:T(128)} %mix_ref.1, bf16[256,4096]{1,0:T(8,128)(2,1)} %hid_hbm.1, bf16[4096,256]{1,0:T(8,128)(2,1)} %kw_hbm.1, bf16[256,1024]{1,0:T(8,128)(2,1)} %q_hbm.1, bf16[256,256]{1,0:T(8,128)(2,1)} %val_hbm.1, ...), custom_call_target="tpu_custom_call" | custom-call | tf_op jit(solution)/shard_map/pallas_call | solution.py:282
  157.6 1.9 %copy.17 = bf16[256,1024]{1,0:T(8,128)(2,1)} copy(bf16[256,1024]{1,0:T(8,128)(2,1)} %get-tuple-element.8) | data formatting | bytes 1048576
  159.5 1.6 copy.18
  161.1 1.6 copy.19
  162.6 1.6 copy.20

commit v2 on v1

v2 whole, which is shorter than its diff:
```python
import functools
import math

import jax
import jax.numpy as jnp
from jax import lax
from jax.experimental import pallas as pl
from jax.experimental.pallas import tpu as pltpu
from jax.sharding import PartitionSpec as P

HEAD_DIM = 128
V_DIM = 256
OUT_SCALE = 0.8
NORM_EPS = 1e-06
LOG2E = math.log2(math.e)
PLANES = 4
MESH_ID = pl.DeviceIdType.MESH
BF16 = jnp.bfloat16
F32 = jnp.float32


def nn(a, b):
    return jnp.dot(a, b, preferred_element_type=F32)


def kernel(n, heads, mix_ref, hid_hbm, kw_hbm, q_hbm, val_hbm, map_hbm, log_hbm, og_hbm, gain_hbm,
           gq_ref, gk_ref, gv_ref, gw_ref,
           hid, kw, maps, logs, og, gain, kb, vb, ktb, qn, dn, qt, dt, stats, dqt, dq_own, dq_out, dq_in,
           ds_a, ds_b, w_a, dk_sum, dv_sum, core_k, core_v, core_k_in, core_v_in, k_out, v_out, k_in, v_in,
           gkt, x_out, x_in, dw_out, dw_in,
           ld, kv_send, kv_recv, f_send, f_recv, q_send, q_recv, r_send, b_send, b_recv,
           c_send, c_recv, t_send, t_recv, y_send, y_recv, w_send, w_recv):
    chips = n // 2
    ny = chips // PLANES
    me = lax.axis_index("sp")
    tp = lax.axis_index("tp")
    u = me // 2
    c = me % 2
    z = u // ny
    y = u % ny
    rows = hid.shape[0]
    scale = HEAD_DIM ** (-0.5)
    partner = 2 * u + 1 - c
    width = hid.shape[1] // n
    passes = PLANES - 1 - z

    barrier = pltpu.get_barrier_semaphore()

    def greet(i, carry):
        peer = 2 * lax.rem(u + i, chips) + c
        pl.semaphore_signal(barrier, inc=1, device_id=(peer, tp), device_id_type=MESH_ID)
        return carry

    lax.fori_loop(1, chips, greet, 0)
    pl.semaphore_signal(barrier, inc=1, device_id=(partner, tp), device_id_type=MESH_ID)

    mine = pl.ds(pl.multiple_of(c * rows, rows), rows)
    other = pl.ds(pl.multiple_of((1 - c) * rows, rows), rows)
    loads = [
        pltpu.make_async_copy(q_hbm, qn.at[z], ld.at[0]),
        pltpu.make_async_copy(val_hbm, vb.at[y, mine, :], ld.at[1]),
        pltpu.make_async_copy(kw_hbm, kw, ld.at[2]),
        pltpu.make_async_copy(hid_hbm, hid, ld.at[3]),
        pltpu.make_async_copy(map_hbm, maps, ld.at[4]),
        pltpu.make_async_copy(og_hbm, og, ld.at[5]),
        pltpu.make_async_copy(gain_hbm, gain, ld.at[6]),
        pltpu.make_async_copy(log_hbm, logs, ld.at[7]),
    ]
    for load in loads:
        load.start()

    def to(src, dst, s_sem, r_sem, device):
        return pltpu.make_async_remote_copy(
            src_ref=src, dst_ref=dst, send_sem=s_sem, recv_sem=r_sem,
            device_id=(device, tp), device_id_type=MESH_ID)

    def at(plane, col):
        return 2 * (plane * ny + col) + c

    def kv_copy(m, buf, source, dest):
        part = buf.at[source, mine, :]
        return to(part, part, kv_send.at[m, dest], kv_recv.at[m, source], at(z, dest))

    def f_copy(m, buf, source):
        part = buf.at[source, mine, :]
        return to(part, part, f_send.at[m, source], f_recv.at[m, source], partner)

    def f_wait(m, buf, source):
        part = buf.at[source, other, :]
        to(part, part, f_send.at[m, source], f_recv.at[m, source], partner).wait_recv()

    def q_copy(m, buf, source, dest, sem):
        return to(buf.at[source], buf.at[source], sem, q_recv.at[m, source], at(dest, y))

    def b_copy(source, dest):
        return to(dq_out.at[dest], dq_in.at[source], b_send.at[dest], b_recv.at[source], at(dest, y))

    def c_copy(m, src, dst, col):
        return to(src.at[col], dst.at[col], c_send.at[m, col], c_recv.at[m, col], partner)

    def t_copy(m, src, dst, source, dest):
        return to(src.at[dest], dst.at[source], t_send.at[m, dest], t_recv.at[m, source], at(z, dest))

    def y_copy(chip):
        return to(x_out.at[chip], x_in.at[chip], y_send.at[chip], y_recv.at[chip], partner)

    def w_copy(dest, source):
        return to(dw_out.at[dest], dw_in.at[source], w_send.at[dest], w_recv.at[source], 2 * dest + c)

    def send_down(m, buf):
        @pl.when(z >= 1)
        def _():
            q_copy(m, buf, z, z - 1, q_send.at[m, 0]).start()

        @pl.when(z == PLANES - 1)
        def _():
            q_copy(m, buf, z, 0, q_send.at[m, 1]).start()

    def others(body):
        def one(i, carry):
            body(lax.rem(y + ny - i, ny))
            return carry

        lax.fori_loop(1, ny, one, 0)

    dk_sum[...] = jnp.zeros_like(dk_sum)
    dv_sum[...] = jnp.zeros_like(dv_sum)
    dqt[...] = jnp.zeros_like(dqt)
    loads[0].wait()
    loads[1].wait()
    pl.semaphore_wait(barrier, chips)
    send_down(0, qn)
    f_copy(1, vb, y).start()
    others(lambda col: kv_copy(1, vb, y, col).start())

    loads[2].wait()
    loads[3].wait()
    kb[y, mine, :] = nn(hid[...], kw[...]).astype(BF16)
    for load in loads[4:]:
        load.wait()
    f_copy(0, kb, y).start()
    others(lambda col: kv_copy(0, kb, y, col).start())

    lane = lax.broadcasted_iota(jnp.int32, (rows, 128), 1)
    terms = jnp.zeros((rows, 128), F32)
    for h in range(heads):
        mix = mix_ref[h]
        first = maps[:, (2 * h) * V_DIM:(2 * h + 1) * V_DIM].astype(F32)
        second = maps[:, (2 * h + 1) * V_DIM:(2 * h + 2) * V_DIM].astype(F32)
        pre = first - mix * second
        inverse = lax.rsqrt(jnp.mean(pre * pre, axis=-1, keepdims=True) + NORM_EPS)
        up = og[:, h * V_DIM:(h + 1) * V_DIM].astype(F32) * gain[...] * OUT_SCALE
        d_out = inverse * (up - pre * (inverse * inverse * jnp.mean(up * pre, axis=-1, keepdims=True)))
        dn[z, :, h * V_DIM:(h + 1) * V_DIM] = d_out.astype(BF16)
        terms = jnp.where(lane == 2 * h, jnp.sum(d_out * first, axis=-1, keepdims=True), terms)
        terms = jnp.where(lane == 2 * h + 1, jnp.sum(d_out * second, axis=-1, keepdims=True), terms)
    stats[z, 2 * heads:4 * heads] = terms.T[:2 * heads]
    mix_row = lax.broadcasted_iota(jnp.int32, (2 * heads, rows), 0)
    log_rows = logs[...] * LOG2E
    for h in range(heads):
        shift = jnp.log(jnp.full((2 * heads, rows), mix_ref[h], F32)) * LOG2E
        log_rows = jnp.where(mix_row == 2 * h + 1, log_rows - shift, log_rows)
    stats[z, :2 * heads] = log_rows

    send_down(1, dn)

    @pl.when(z == PLANES - 1)
    def _():
        q_copy(1, dn, z, 1, q_send.at[1, 2]).start()

    def s_copy(source, dest):
        return q_copy(2, stats, source, dest, q_send.at[2, dest])

    def send_stats(dest, carry):
        s_copy(z, dest).start()
        return carry

    lax.fori_loop(0, z, send_stats, 0)

    def turn(plane):
        for h in range(2 * heads):
            qt[h * HEAD_DIM:(h + 1) * HEAD_DIM, :] = qn[plane, :, h * HEAD_DIM:(h + 1) * HEAD_DIM].T
        for h in range(heads):
            dt[h * V_DIM:(h + 1) * V_DIM, :] = dn[plane, :, h * V_DIM:(h + 1) * V_DIM].T

    k_rows = 2 * rows

    def block(col, plane, masked):
        def products(h):
            kk = kb.at[col]
            s_a = nn(kk[:, :HEAD_DIM], qt[(2 * h) * HEAD_DIM:(2 * h + 1) * HEAD_DIM, :])
            s_b = nn(kk[:, HEAD_DIM:], qt[(2 * h + 1) * HEAD_DIM:(2 * h + 2) * HEAD_DIM, :])
            d_p = nn(vb[col], dt[h * V_DIM:(h + 1) * V_DIM, :])
            return s_a, s_b, d_p

        ready = products(0)
        for h in range(heads):
            s_a, s_b, d_p = ready
            if h + 1 < heads:
                ready = products(h + 1)
            x_a = s_a * (scale * LOG2E) - stats[plane, 2 * h:2 * h + 1, :]
            x_b = s_b * (scale * LOG2E) - stats[plane, 2 * h + 1:2 * h + 2, :]
            if masked:
                key_at = lax.broadcasted_iota(jnp.int32, (k_rows, rows), 0)
                query_at = c * rows + lax.broadcasted_iota(jnp.int32, (k_rows, rows), 1)
                seen = key_at <= query_at
                x_a = jnp.where(seen, x_a, -1e30)
                x_b = jnp.where(seen, x_b, -1e30)
            p_a = jnp.exp2(x_a)
            p_b = jnp.exp2(x_b)
            cols = slice(h * rows, (h + 1) * rows)
            a_h = (p_a * (d_p - stats[plane, 2 * heads + 2 * h:2 * heads + 2 * h + 1, :])).astype(BF16)
            b_h = (p_b * (stats[plane, 2 * heads + 2 * h + 1:2 * heads + 2 * h + 2, :] - d_p)).astype(BF16)
            w_a[:, cols] = (p_a - p_b).astype(BF16)
            ds_a[:, cols] = a_h
            ds_b[:, cols] = b_h
            dqt[(2 * h) * HEAD_DIM:(2 * h + 1) * HEAD_DIM, :] += nn(ktb[col, :HEAD_DIM, :], a_h)
            dqt[(2 * h + 1) * HEAD_DIM:(2 * h + 2) * HEAD_DIM, :] += nn(ktb[col, HEAD_DIM:, :], b_h)
        g_v = jnp.zeros((k_rows, V_DIM), F32)
        g_a = jnp.zeros((k_rows, HEAD_DIM), F32)
        g_b = jnp.zeros((k_rows, HEAD_DIM), F32)
        for h in range(heads):
            cols = slice(h * rows, (h + 1) * rows)
            g_a += nn(ds_a[:, cols], qn[plane, :, (2 * h) * HEAD_DIM:(2 * h + 1) * HEAD_DIM])
            g_b += nn(ds_b[:, cols], qn[plane, :, (2 * h + 1) * HEAD_DIM:(2 * h + 2) * HEAD_DIM])
            g_v += nn(w_a[:, cols], dn[plane, :, h * V_DIM:(h + 1) * V_DIM])
        dk_sum[col, :, :HEAD_DIM] += g_a
        dk_sum[col, :, HEAD_DIM:] += g_b
        dv_sum[col] += g_v

    turn(z)
    f_wait(0, kb, y)
    f_wait(1, vb, y)
    ktb[y] = kb[y].T
    block(y, z, True)

    def take(i, carry):
        col = lax.rem(y + ny - i, ny)
        for m, buf in ((0, kb), (1, vb)):
            kv_copy(m, buf, col, y).wait_recv()
            f_copy(m, buf, col).start()
        for m, buf in ((0, kb), (1, vb)):
            f_wait(m, buf, col)
        ktb[col] = kb[col].T

        @pl.when(col < y)
        def _():
            block(col, z, False)

        return carry

    lax.fori_loop(1, ny, take, 0)
    dq_own[...] = dqt[...]

    def to_partner(col):
        core_k[col] = dk_sum[col, other, :].astype(BF16)
        c_copy(0, core_k, core_k_in, col).start()
        core_v[col] = dv_sum[col, other, :].astype(BF16)
        c_copy(1, core_v, core_v_in, col).start()

    def to_owner(col):
        c_copy(0, core_k, core_k_in, col).wait_recv()
        k_out[col] = (dk_sum[col, mine, :] + core_k_in[col].astype(F32)).astype(BF16)
        t_copy(0, k_out, k_in, y, col).start()
        c_copy(1, core_v, core_v_in, col).wait_recv()
        v_out[col] = (dv_sum[col, mine, :] + core_v_in[col].astype(F32)).astype(BF16)
        t_copy(1, v_out, v_in, y, col).start()

    def one_pass(p, carry):
        plane = jnp.where((z == 0) & (p >= 2), PLANES + 1 - p, z + p)
        q_copy(0, qn, plane, z, q_send.at[0, 0]).wait_recv()

        @pl.when((z >= 1) & (p == 1) & (z <= PLANES - 2))
        def _():
            q_copy(0, qn, plane, z - 1, r_send.at[0]).start()

        q_copy(1, dn, plane, z, q_send.at[1, 0]).wait_recv()

        @pl.when((z == 1) & (p == 1))
        def _():
            q_copy(1, dn, plane, z - 1, r_send.at[1]).start()

        q_copy(2, stats, plane, z, q_send.at[2, 0]).wait_recv()
        turn(plane)
        dqt[...] = jnp.zeros_like(dqt)

        def one(i, inner):
            col = lax.rem(y + i, ny)
            block(col, plane, False)

            @pl.when(p == passes)
            def _():
                @pl.when(i > 1)
                def _():
                    to_owner(lax.rem(y + i - 1, ny))

                to_partner(col)

            return inner

        lax.fori_loop(1, ny + 1, one, 0)
        dq_out[plane] = dqt[...].astype(BF16)
        b_copy(z, plane).start()
        return carry

    lax.fori_loop(1, passes + 1, one_pass, 0)

    @pl.when(passes == 0)
    def _():
        def give(col, carry):
            to_partner(col)
            return carry

        lax.fori_loop(0, y + 1, give, 0)

        def pass_on(col, carry):
            to_owner(col)
            return carry

        lax.fori_loop(0, y, pass_on, 0)

    c_copy(0, core_k, core_k_in, y).wait_recv()
    gk = dk_sum[y, mine, :] + core_k_in[y].astype(F32)
    first_in = jnp.where(passes == 0, y + 1, 0)

    def add_k(col, total):
        t_copy(0, k_out, k_in, col, y).wait_recv()
        return total + k_in[col].astype(F32)

    gk = lax.fori_loop(first_in, y, add_k, gk)
    gk = lax.fori_loop(y + 1, ny, add_k, gk) * scale
    gk_ref[...] = gk.astype(BF16)
    gkt[...] = gk.T.astype(BF16)

    def project(i, carry):
        chip = lax.rem(u + 1 + i, chips)
        piece = nn(gkt[...], hid[:, pl.ds(pl.multiple_of(2 * width * chip, 2 * width), 2 * width)])
        low, high = piece[:, :width], piece[:, width:]
        dw_out[chip] = jnp.where(c == 0, low, high).astype(BF16)
        x_out[chip] = jnp.where(c == 0, high, low).astype(BF16)
        y_copy(chip).start()
        return carry

    lax.fori_loop(0, chips, project, 0)

    def spread(i, carry):
        chip = lax.rem(u + 1 + i, chips)
        y_copy(chip).wait_recv()
        dw_out[chip] = (dw_out[chip].astype(F32) + x_in[chip].astype(F32)).astype(BF16)

        @pl.when(chip != u)
        def _():
            w_copy(chip, u).start()

        return carry

    lax.fori_loop(0, chips, spread, 0)

    c_copy(1, core_v, core_v_in, y).wait_recv()
    gv = dv_sum[y, mine, :] + core_v_in[y].astype(F32)

    def add_v(col, total):
        t_copy(1, v_out, v_in, col, y).wait_recv()
        return total + v_in[col].astype(F32)

    gv = lax.fori_loop(first_in, y, add_v, gv)
    gv = lax.fori_loop(y + 1, ny, add_v, gv)
    gv_ref[...] = gv.astype(BF16)

    def add_q(plane, carry):
        b_copy(plane, z).wait_recv()
        dq_own[...] += dq_in[plane].astype(F32)
        return carry

    lax.fori_loop(0, z, add_q, 0)
    for h in range(2 * heads):
        part = dq_own[h * HEAD_DIM:(h + 1) * HEAD_DIM, :]
        gq_ref[:, h * HEAD_DIM:(h + 1) * HEAD_DIM] = (part * scale).T.astype(BF16)

    def add_w(i, total):
        chip = chips - 1 - i
        w_copy(u, chip).wait_recv()
        return total + dw_in[chip].astype(F32)

    total = dw_out[u].astype(F32)
    total = lax.fori_loop(0, chips - 1 - u, add_w, total)
    total = lax.fori_loop(chips - u, chips, add_w, total)
    gw_ref[...] = total.T

    for m, buf in ((0, kb), (1, vb)):
        f_copy(m, buf, y).wait_send()

    def sent(col):
        for m, buf in ((0, kb), (1, vb)):
            kv_copy(m, buf, y, col).wait_send()
            f_copy(m, buf, col).wait_send()

    others(sent)

    @pl.when(z >= 1)
    def _():
        q_copy(0, qn, z, 0, q_send.at[0, 0]).wait_send()
        q_copy(1, dn, z, 0, q_send.at[1, 0]).wait_send()

    @pl.when(z == PLANES - 1)
    def _():
        q_copy(0, qn, z, 0, q_send.at[0, 1]).wait_send()
        q_copy(1, dn, z, 0, q_send.at[1, 1]).wait_send()
        q_copy(1, dn, z, 0, q_send.at[1, 2]).wait_send()

    @pl.when((z >= 1) & (z <= PLANES - 2))
    def _():
        q_copy(0, qn, z + 1, z - 1, r_send.at[0]).wait_send()

    @pl.when(z == 1)
    def _():
        q_copy(1, dn, z + 1, z - 1, r_send.at[1]).wait_send()

    def stats_sent(dest, carry):
        s_copy(z, dest).wait_send()
        return carry

    lax.fori_loop(0, z, stats_sent, 0)

    def back_sent(plane, carry):
        b_copy(z, plane).wait_send()
        return carry

    lax.fori_loop(z + 1, PLANES, back_sent, 0)
    last_in = jnp.where(passes == 0, y + 1, ny)

    def terms_sent(col, carry):
        for m, src, dst in ((0, core_k, core_k_in), (1, core_v, core_v_in)):
            c_copy(m, src, dst, col).wait_send()

        @pl.when(col != y)
        def _():
            t_copy(0, k_out, k_in, y, col).wait_send()
            t_copy(1, v_out, v_in, y, col).wait_send()

        return carry

    lax.fori_loop(0, last_in, terms_sent, 0)

    def dw_sent(chip, carry):
        y_copy(chip).wait_send()

        @pl.when(chip != u)
        def _():
            w_copy(chip, u).wait_send()

        return carry

    lax.fori_loop(0, chips, dw_sent, 0)


def on_device(n, hidden, key_weight, queries, values, map_out, log_sums, out_grad, mixing, out_gain):
    rows, model = hidden.shape
    heads = mixing.shape[0]
    k_cols = key_weight.shape[1]
    q_cols = queries.shape[1]
    chips = n // 2
    ny = chips // PLANES
    width = model // n
    vm = pltpu.VMEM
    dma = pltpu.SemaphoreType.DMA
    anywhere = pl.BlockSpec(memory_space=pl.ANY)
    inside = pl.BlockSpec(memory_space=pltpu.VMEM)
    tall = vm((2 * rows, heads * rows), BF16)
    slots = vm((ny, rows, k_cols), BF16)
    return pl.pallas_call(
        functools.partial(kernel, n, heads),
        out_shape=(
            jax.ShapeDtypeStruct((rows, q_cols), BF16),
            jax.ShapeDtypeStruct((rows, k_cols), BF16),
            jax.ShapeDtypeStruct((rows, V_DIM), BF16),
            jax.ShapeDtypeStruct((width, k_cols), F32),
        ),
        in_specs=[pl.BlockSpec(memory_space=pltpu.SMEM)] + [anywhere] * 8,
        out_specs=(inside,) * 4,
        scratch_shapes=[
            vm((rows, model), BF16),
            vm((model, k_cols), BF16),
            vm((rows, 2 * heads * V_DIM), BF16),
            vm((2 * heads, rows), F32),
            vm((rows, heads * V_DIM), BF16),
            vm((1, V_DIM), F32),
            vm((ny, 2 * rows, k_cols), BF16),
            vm((ny, 2 * rows, V_DIM), BF16),
            vm((ny, k_cols, 2 * rows), BF16),
            vm((PLANES, rows, q_cols), BF16),
            vm((PLANES, rows, heads * V_DIM), BF16),
            vm((q_cols, rows), BF16),
            vm((heads * V_DIM, rows), BF16),
            vm((PLANES, 4 * heads, rows), F32),
            vm((q_cols, rows), F32),
            vm((q_cols, rows), F32),
            vm((PLANES, q_cols, rows), BF16),
            vm((PLANES, q_cols, rows), BF16),
            tall, tall, tall,
            vm((ny, 2 * rows, k_cols), F32),
            vm((ny, 2 * rows, V_DIM), F32),
            slots, slots, slots, slots, slots, slots, slots, slots,
            vm((k_cols, rows), BF16),
            vm((chips, k_cols, width), BF16),
            vm((chips, k_cols, width), BF16),
            vm((chips, k_cols, width), BF16),
            vm((chips, k_cols, width), BF16),
            dma((8,)),
            dma((2, ny)), dma((2, ny)),
            dma((2, ny)), dma((2, ny)),
            dma((3, PLANES)), dma((3, PLANES)), dma((2,)),
            dma((PLANES,)), dma((PLANES,)),
            dma((2, ny)), dma((2, ny)),
            dma((2, ny)), dma((2, ny)),
            dma((chips,)), dma((chips,)),
            dma((chips,)), dma((chips,)),
        ],
        compiler_params=pltpu.CompilerParams(
            collective_id=0, has_side_effects=True, vmem_limit_bytes=63 * 1024 * 1024),
    )(mixing, hidden, key_weight, queries, values, map_out, log_sums, out_grad, out_gain.reshape(1, -1))


def solution(mesh):
    placed = (
        P("sp", None),
        P(None, "tp"),
        P("sp", "tp"),
        P("sp", "tp"),
        P("sp", "tp"),
        P("tp", "sp"),
        P("sp", "tp"),
        P("tp"),
        P(),
    )
    return jax.shard_map(
        functools.partial(on_device, mesh.shape["sp"]),
        mesh=mesh,
        in_specs=placed,
        out_specs=(P("sp", "tp"), P("sp", "tp"), P("sp", "tp"), P("sp", "tp")),
        check_vma=False,
    )
```

time: 164 us -> 107 us (0.65)
  the two profiles are of different devices: /device:TPU:81 before, /device:TPU:1 now
where the time goes in v2:
time: 107 us
  Pallas kernels  99.4 us (93%)
  local copies, waits for them, and re-layouts  6.57 us (6%)
    pallas_call x1, Pallas kernels, on_device(): pl.pallas_call(functools.partial(kernel, n, heads), out_shape=(jax.ShapeD...  99.4 us
    unnamed x4, local copies, waits for them, and re-layouts  6.57 us

profile of v2, /device:TPU:1, one launch (start us, length us, event | category | flops | bytes accessed | tf_op | source)
XLA Modules:
  0.0 106.6 jit_solution(16874333792405155936)
XLA Ops:
  0.6 99.4 %shard_map.120 = (bf16[256,1024]{1,0:T(8,128)(2,1)}, bf16[256,256]{1,0:T(8,128)(2,1)}, bf16[256,256]{1,0:T(8,128)(2,1)}, f32[128,256]{1,0:T(8,128)}) custom-call(f32[4]{0:T(128)} %mix_ref.1, bf16[256,4096]{1,0:T(8,128)(2,1)} %hid_hbm.1, bf16[4096,256]{1,0:T(8,128)(2,1)} %kw_hbm.1, bf16[256,1024]{1,0:T(8,128)(2,1)} %q_hbm.1, bf16[256,256]{1,0:T(8,128)(2,1)} %val_hbm.1, ...), custom_call_target="tpu_custom_call" | custom-call | tf_op jit(solution)/shard_map/pallas_call | solution.py:471
  100.1 1.9 %copy.17 = bf16[256,1024]{1,0:T(8,128)(2,1)} copy(bf16[256,1024]{1,0:T(8,128)(2,1)} %get-tuple-element.8) | data formatting | bytes 1048576
  101.9 1.6 %copy.18 = bf16[256,256]{1,0:T(8,128)(2,1)} copy(bf16[256,256]{1,0:T(8,128)(2,1)} %get-tuple-element.9) | data formatting | bytes 262144
  103.5 1.6 %copy.19 = bf16[256,256]{1,0:T(8,128)(2,1)} copy(bf16[256,256]{1,0:T(8,128)(2,1)} %get-tuple-element.10) | data formatting | bytes 262144
  105.1 1.6 %copy.20 = f32[128,256]{1,0:T(8,128)} copy(f32[128,256]{1,0:T(8,128)} %get-tuple-element.11) | data formatting | bytes 262144

commit v3 on v2

v3 whole, which is shorter than its diff:
```python
import functools
import math

import jax
import jax.numpy as jnp
from jax import lax
from jax.experimental import pallas as pl
from jax.experimental.pallas import tpu as pltpu
from jax.sharding import PartitionSpec as P

HEAD_DIM = 128
V_DIM = 256
OUT_SCALE = 0.8
NORM_EPS = 1e-06
LOG2E = math.log2(math.e)
PLANES = 4
LAG = 3
MESH_ID = pl.DeviceIdType.MESH
BF16 = jnp.bfloat16
F32 = jnp.float32


def nn(a, b):
    return jnp.dot(a, b, preferred_element_type=F32)


def write_out(a, b, c, d, a_out, b_out, c_out, d_out, sem):
    copies = [pltpu.make_async_copy(src, dst, sem.at[i])
              for i, (src, dst) in enumerate(((a, a_out), (b, b_out), (c, c_out), (d, d_out)))]
    for copy in copies:
        copy.start()
    for copy in copies:
        copy.wait()


def kernel(n, heads, mix_ref, hid_hbm, kw_hbm, q_hbm, val_hbm, map_hbm, log_hbm, og_hbm, gain_hbm,
           gq_ref, gk_ref, gv_ref, gw_ref,
           hid, kw, maps, logs, og, gain, kb, vb, ktb, qn, dn, qt, dt, stats, dqt, dq_own, dq_out, dq_in,
           ds_a, ds_b, w_a, dk_sum, dv_sum, core_k, core_v, core_k_in, core_v_in, k_out, v_out, k_in, v_in,
           gkt, x_out, x_in, dw_out, dw_in, e_out, e_in, own_k, own_v, ring_in,
           ld, kv_send, kv_recv, f_send, f_recv, q_send, q_recv, r_send, b_send, b_recv,
           c_send, c_recv, t_send, t_recv, y_send, y_recv, w_send, w_recv,
           h_send, h_recv, e_send, e_recv, g_send, g_recv, p_send, p_recv):
    chips = n // 2
    ny = chips // PLANES
    ring = ny == 4
    me = lax.axis_index("sp")
    tp = lax.axis_index("tp")
    u = me // 2
    c = me % 2
    z = u // ny
    y = u % ny
    rows = hid.shape[0]
    scale = HEAD_DIM ** (-0.5)
    partner = 2 * u + 1 - c
    width = hid.shape[1] // n
    odd = lax.rem(z, 2) == 1
    top = z == PLANES - 1
    low = z < PLANES // 2
    n_q = jnp.where(z == 0, 2, jnp.where(z == PLANES - 1, 0, 1))
    above = jnp.where(low, 2 * z + 1, z)
    below = lax.div(z, 2)

    barrier = pltpu.get_barrier_semaphore()

    def greet(i, carry):
        peer = 2 * lax.rem(u + i, chips) + c
        pl.semaphore_signal(barrier, inc=1, device_id=(peer, tp), device_id_type=MESH_ID)
        return carry

    lax.fori_loop(1, chips, greet, 0)
    pl.semaphore_signal(barrier, inc=1, device_id=(partner, tp), device_id_type=MESH_ID)

    mine = pl.ds(pl.multiple_of(c * rows, rows), rows)
    other = pl.ds(pl.multiple_of((1 - c) * rows, rows), rows)
    loads = [
        pltpu.make_async_copy(q_hbm, qn.at[z], ld.at[0]),
        pltpu.make_async_copy(map_hbm, maps, ld.at[1]),
        pltpu.make_async_copy(og_hbm, og, ld.at[2]),
        pltpu.make_async_copy(gain_hbm, gain, ld.at[3]),
        pltpu.make_async_copy(log_hbm, logs, ld.at[4]),
        pltpu.make_async_copy(val_hbm, vb.at[y, mine, :], ld.at[5]),
        pltpu.make_async_copy(kw_hbm, kw, ld.at[6]),
        pltpu.make_async_copy(hid_hbm, hid, ld.at[7]),
    ]
    for load in loads:
        load.start()

    def to(src, dst, s_sem, r_sem, device):
        return pltpu.make_async_remote_copy(
            src_ref=src, dst_ref=dst, send_sem=s_sem, recv_sem=r_sem,
            device_id=(device, tp), device_id_type=MESH_ID)

    def at(plane, col):
        return 2 * (plane * ny + col) + c

    def kv_copy(m, buf, source, dest):
        part = buf.at[source, mine, :]
        return to(part, part, kv_send.at[m, source - y + dest], kv_recv.at[m, source], at(z, dest))

    def kv_wait(m, buf, slot):
        part = buf.at[slot, mine, :]
        to(part, part, kv_send.at[m, 0], kv_recv.at[m, slot], me).wait_recv()

    def turned(step):
        return lax.rem(y + step, ny)

    def g_copy(m, buf, s, step):
        part = buf.at[s * ny + turned(4 - step), mine, :]
        return to(part, part, g_send.at[m, s], kv_recv.at[m, s * ny + turned(4 - step)], at(z, turned(step)))

    def p_copy(m, src, s, step):
        return to(src.at[s * ny + turned(2)], ring_in.at[m, s], p_send.at[m, s], p_recv.at[m, s],
                  at(z, turned(step)))

    def near(body):
        if ring:
            body(turned(1))
            body(turned(3))
        else:
            others(body)

    def h_copy(m, buf):
        return to(buf.at[y, mine, :], buf.at[ny + y, mine, :], h_send.at[m], h_recv.at[m], at(above, y))

    def e_copy(m):
        return to(e_out.at[m], e_in.at[m], e_send.at[m], e_recv.at[m], at(below, y))

    def f_copy(m, buf, source):
        part = buf.at[source, mine, :]
        return to(part, part, f_send.at[m, source], f_recv.at[m, source], partner)

    def f_wait(m, buf, source):
        part = buf.at[source, other, :]
        to(part, part, f_send.at[m, source], f_recv.at[m, source], partner).wait_recv()

    def q_copy(m, buf, source, dest, sem):
        return to(buf.at[source], buf.at[source], sem, q_recv.at[m, source], at(dest, y))

    def b_copy(source, dest):
        return to(dq_out.at[dest], dq_in.at[source], b_send.at[dest], b_recv.at[source], at(dest, y))

    def c_copy(m, src, dst, col):
        return to(src.at[col], dst.at[col], c_send.at[m, col], c_recv.at[m, col], partner)

    def t_copy(m, src, dst, base, source, dest):
        return to(src.at[base + dest], dst.at[base + source], t_send.at[m, base + dest],
                  t_recv.at[m, base + source], at(z, dest))

    def y_copy(chip):
        return to(x_out.at[chip], x_in.at[chip], y_send.at[chip], y_recv.at[chip], partner)

    def w_copy(dest, source):
        return to(dw_out.at[dest], dw_in.at[source], w_send.at[dest], w_recv.at[source], 2 * dest + c)

    def send_down(m, buf):
        @pl.when(z >= 2)
        def _():
            q_copy(m, buf, z, z - 1, q_send.at[m, 0]).start()

        @pl.when(z == PLANES - 1)
        def _():
            q_copy(m, buf, z, 0, q_send.at[m, 1]).start()

    def others(body):
        def one(i, carry):
            body(lax.rem(y + ny - i, ny))
            return carry

        lax.fori_loop(1, ny, one, 0)

    dk_sum[...] = jnp.zeros_like(dk_sum)
    dv_sum[...] = jnp.zeros_like(dv_sum)
    dqt[...] = jnp.zeros_like(dqt)
    loads[0].wait()
    pl.semaphore_wait(barrier, chips)
    send_down(0, qn)
    for load in loads[1:5]:
        load.wait()

    lane = lax.broadcasted_iota(jnp.int32, (rows, 128), 1)
    terms = jnp.zeros((rows, 128), F32)
    for h in range(heads):
        mix = mix_ref[h]
        first = maps[:, (2 * h) * V_DIM:(2 * h + 1) * V_DIM].astype(F32)
        second = maps[:, (2 * h + 1) * V_DIM:(2 * h + 2) * V_DIM].astype(F32)
        pre = first - mix * second
        inverse = lax.rsqrt(jnp.mean(pre * pre, axis=-1, keepdims=True) + NORM_EPS)
        up = og[:, h * V_DIM:(h + 1) * V_DIM].astype(F32) * gain[...] * OUT_SCALE
        d_out = inverse * (up - pre * (inverse * inverse * jnp.mean(up * pre, axis=-1, keepdims=True)))
        dn[z, :, h * V_DIM:(h + 1) * V_DIM] = d_out.astype(BF16)
        terms = jnp.where(lane == 2 * h, jnp.sum(d_out * first, axis=-1, keepdims=True), terms)
        terms = jnp.where(lane == 2 * h + 1, jnp.sum(d_out * second, axis=-1, keepdims=True), terms)
    stats[z, 2 * heads:4 * heads] = terms.T[:2 * heads]
    mix_row = lax.broadcasted_iota(jnp.int32, (2 * heads, rows), 0)
    log_rows = logs[...] * LOG2E
    for h in range(heads):
        shift = jnp.log(jnp.full((2 * heads, rows), mix_ref[h], F32)) * LOG2E
        log_rows = jnp.where(mix_row == 2 * h + 1, log_rows - shift, log_rows)
    stats[z, :2 * heads] = log_rows

    send_down(1, dn)

    @pl.when(z >= 2)
    def _():
        q_copy(2, stats, z, z - 1, q_send.at[2, 1]).start()
        q_copy(2, stats, z, 0, q_send.at[2, 0]).start()

    def share(m, buf):
        f_copy(m, buf, y).start()

        @pl.when(low)
        def _():
            h_copy(m, buf).start()

        near(lambda col: kv_copy(m, buf, y, col).start())

    loads[5].wait()
    share(1, vb)
    loads[6].wait()
    loads[7].wait()
    kb[y, mine, :] = nn(hid[...], kw[...]).astype(BF16)
    share(0, kb)

    def turn(plane):
        for h in range(2 * heads):
            qt[h * HEAD_DIM:(h + 1) * HEAD_DIM, :] = qn[plane, :, h * HEAD_DIM:(h + 1) * HEAD_DIM].T
        for h in range(heads):
            dt[h * V_DIM:(h + 1) * V_DIM, :] = dn[plane, :, h * V_DIM:(h + 1) * V_DIM].T

    k_rows = 2 * rows

    def block(col, plane, masked):
        def products(h):
            kk = kb.at[col]
            s_a = nn(kk[:, :HEAD_DIM], qt[(2 * h) * HEAD_DIM:(2 * h + 1) * HEAD_DIM, :])
            s_b = nn(kk[:, HEAD_DIM:], qt[(2 * h + 1) * HEAD_DIM:(2 * h + 2) * HEAD_DIM, :])
            d_p = nn(vb[col], dt[h * V_DIM:(h + 1) * V_DIM, :])
            return s_a, s_b, d_p

        ready = products(0)
        for h in range(heads):
            s_a, s_b, d_p = ready
            if h + 1 < heads:
                ready = products(h + 1)
            x_a = s_a * (scale * LOG2E) - stats[plane, 2 * h:2 * h + 1, :]
            x_b = s_b * (scale * LOG2E) - stats[plane, 2 * h + 1:2 * h + 2, :]
            if masked:
                key_at = lax.broadcasted_iota(jnp.int32, (k_rows, rows), 0)
                query_at = c * rows + lax.broadcasted_iota(jnp.int32, (k_rows, rows), 1)
                seen = key_at <= query_at
                x_a = jnp.where(seen, x_a, -1e30)
                x_b = jnp.where(seen, x_b, -1e30)
            p_a = jnp.exp2(x_a)
            p_b = jnp.exp2(x_b)
            cols = slice(h * rows, (h + 1) * rows)
            a_h = (p_a * (d_p - stats[plane, 2 * heads + 2 * h:2 * heads + 2 * h + 1, :])).astype(BF16)
            b_h = (p_b * (stats[plane, 2 * heads + 2 * h + 1:2 * heads + 2 * h + 2, :] - d_p)).astype(BF16)
            w_a[:, cols] = (p_a - p_b).astype(BF16)
            ds_a[:, cols] = a_h
            ds_b[:, cols] = b_h
            dqt[(2 * h) * HEAD_DIM:(2 * h + 1) * HEAD_DIM, :] += nn(ktb[col, :HEAD_DIM, :], a_h)
            dqt[(2 * h + 1) * HEAD_DIM:(2 * h + 2) * HEAD_DIM, :] += nn(ktb[col, HEAD_DIM:, :], b_h)
        g_v = jnp.zeros((k_rows, V_DIM), F32)
        g_a = jnp.zeros((k_rows, HEAD_DIM), F32)
        g_b = jnp.zeros((k_rows, HEAD_DIM), F32)
        for h in range(heads):
            cols = slice(h * rows, (h + 1) * rows)
            g_a += nn(ds_a[:, cols], qn[plane, :, (2 * h) * HEAD_DIM:(2 * h + 1) * HEAD_DIM])
            g_b += nn(ds_b[:, cols], qn[plane, :, (2 * h + 1) * HEAD_DIM:(2 * h + 2) * HEAD_DIM])
            g_v += nn(w_a[:, cols], dn[plane, :, h * V_DIM:(h + 1) * V_DIM])
        dk_sum[col, :, :HEAD_DIM] += g_a
        dk_sum[col, :, HEAD_DIM:] += g_b
        dv_sum[col] += g_v

    turn(z)
    f_wait(0, kb, y)
    f_wait(1, vb, y)
    ktb[y] = kb[y].T
    block(y, z, True)

    def pass_down(m, buf):
        q_copy(m, buf, z + 1, z, q_send.at[m, 0]).wait_recv()
        q_copy(m, buf, z + 1, z - 1, r_send.at[m]).start()

    def receive(slot):
        for m, buf in ((0, kb), (1, vb)):
            kv_wait(m, buf, slot)
            f_copy(m, buf, slot).start()

    def ready_slot(slot):
        for m, buf in ((0, kb), (1, vb)):
            f_wait(m, buf, slot)
        ktb[slot] = kb[slot].T

    def pass_round(s):
        if ring:
            for m, buf, step in ((0, kb, 3), (1, vb, 1)):
                kv_wait(m, buf, s * ny + turned(4 - step))
                g_copy(m, buf, s, step).start()
                f_copy(m, buf, s * ny + turned(4 - step)).start()
            for m, buf, step in ((0, kb, 3), (1, vb, 1)):
                kv_wait(m, buf, s * ny + turned(step))
                f_copy(m, buf, s * ny + turned(step)).start()

    def far(i):
        if ring:
            return turned(jnp.where(i == 1, 3, jnp.where(i == 2, 1, 2)))
        return turned(ny - i)

    def got(i, slot):
        if ring:
            @pl.when(i == 3)
            def _():
                receive(slot)
        else:
            receive(slot)

    def last_order(i):
        if ring:
            return turned(jnp.where(i == 1, 2, jnp.where(i == 2, 1, jnp.where(i == 3, 3, 0))))
        return turned(i)

    @pl.when(z == 1)
    def _():
        pass_down(0, qn)

    pass_round(0)

    @pl.when(odd)
    def _():
        for m, buf in ((0, kb), (1, vb)):
            to(buf.at[y, mine, :], buf.at[ny + y, mine, :], h_send.at[m], h_recv.at[m], partner).wait_recv()
            f_copy(m, buf, ny + y).start()
            near(lambda col: kv_copy(m, buf, ny + y, col).start())

    def take(i, carry):
        col = far(i)
        got(i, col)
        ready_slot(col)

        @pl.when(col < y)
        def _():
            block(col, z, False)

        return carry

    lax.fori_loop(1, ny, take, 0)
    dq_own[...] = dqt[...]

    @pl.when(odd)
    def _():
        pass_round(1)

    def to_partner(slot):
        core_k[slot] = dk_sum[slot, other, :].astype(BF16)
        c_copy(0, core_k, core_k_in, slot).start()
        core_v[slot] = dv_sum[slot, other, :].astype(BF16)
        c_copy(1, core_v, core_v_in, slot).start()

    def to_owner(base, col):
        slot = base + col
        c_copy(0, core_k, core_k_in, slot).wait_recv()
        k_out[slot] = (dk_sum[slot, mine, :] + core_k_in[slot].astype(F32)).astype(BF16)
        t_copy(0, k_out, k_in, base, y, col).start()
        c_copy(1, core_v, core_v_in, slot).wait_recv()
        v_out[slot] = (dv_sum[slot, mine, :] + core_v_in[slot].astype(F32)).astype(BF16)
        t_copy(1, v_out, v_in, base, y, col).start()

    def to_ring(s, col):
        slot = s * ny + col
        back = lax.rem(col - y + ny, ny)
        for m, sums, core, core_in, out, arrived, step in (
                (0, dk_sum, core_k, core_k_in, k_out, k_in, 3), (1, dv_sum, core_v, core_v_in, v_out, v_in, 1)):
            c_copy(m, core, core_in, slot).wait_recv()
            term = sums[slot, mine, :] + core_in[slot].astype(F32)

            @pl.when(back == step)
            def _():
                p_copy(m, out, s, 4 - step).wait_recv()
                out[slot] = (term + ring_in[m, s].astype(F32)).astype(BF16)

            @pl.when(back != step)
            def _():
                out[slot] = term.astype(BF16)

            @pl.when(back == 2)
            def _():
                p_copy(m, out, s, step).start()

            @pl.when(back != 2)
            def _():
                t_copy(m, out, arrived, s * ny, y, col).start()

    def hand_over(s, col):
        if ring:
            to_ring(s, col)
        else:
            to_owner(s * ny, col)

    @pl.when(top)
    def _():
        def give(col, carry):
            to_partner(col)
            return carry

        lax.fori_loop(0, y + 1, give, 0)

        def pass_on(col, carry):
            to_owner(0, col)
            return carry

        lax.fori_loop(0, y, pass_on, 0)

    first_in = jnp.where(top, y + 1, 0)

    def collect(m, sums, core_in, arrived, src, base, first, whole):
        slot = base + y
        c_copy(m, src, core_in, slot).wait_recv()
        total = sums[slot, mine, :] + core_in[slot].astype(F32)

        def add(col, total):
            t_copy(m, src, arrived, base, col, y).wait_recv()
            return total + arrived[base + col].astype(F32)

        if ring and whole:
            return add(turned(3), add(turned(1), total))
        total = lax.fori_loop(first, y, add, total)
        return lax.fori_loop(y + 1, ny, add, total)

    def extra():
        turn(z)
        dqt[...] = jnp.zeros_like(dqt)

        def one(i, carry):
            col = turned(jnp.where(i == 0, 0, jnp.where(i == 1, 2, jnp.where(i == 2, 1, 3)))) if ring else turned(i)
            prev = turned(jnp.where(i == 2, 2, 1)) if ring else turned(i - 1)
            slot = ny + col

            if ring:
                @pl.when(i == 1)
                def _():
                    receive(slot)
            else:
                @pl.when(i > 0)
                def _():
                    receive(slot)

            @pl.when((z == 1) & (i == 1 % ny))
            def _():
                pass_down(1, dn)

            ready_slot(slot)
            block(slot, z, False)

            @pl.when(i > 1)
            def _():
                hand_over(1, prev)

            to_partner(slot)
            return carry

        lax.fori_loop(0, ny, one, 0)
        if ny > 1:
            hand_over(1, turned(ny - 1))
        dq_own[...] += dqt[...]
        e_out[0] = collect(0, dk_sum, core_k_in, k_in, core_k, ny, 0, True).astype(BF16)
        e_copy(0).start()
        e_out[1] = collect(1, dv_sum, core_v_in, v_in, core_v, ny, 0, True).astype(BF16)
        e_copy(1).start()

    @pl.when(odd)
    def _():
        extra()

    def one_pass(p, carry):
        plane = jnp.where(z == 0, PLANES - p, z + 1)

        @pl.when(z != 1)
        def _():
            q_copy(0, qn, plane, z, q_send.at[0, 0]).wait_recv()
            q_copy(1, dn, plane, z, q_send.at[1, 0]).wait_recv()

        q_copy(2, stats, plane, z, q_send.at[2, 0]).wait_recv()
        turn(plane)
        dqt[...] = jnp.zeros_like(dqt)

        def one(i, inner):
            col = last_order(i)
            block(col, plane, False)

            @pl.when(p == n_q)
            def _():
                @pl.when(i > 1)
                def _():
                    hand_over(0, last_order(i - 1))

                to_partner(col)

            return inner

        lax.fori_loop(1, ny + 1, one, 0)
        dq_out[plane] = dqt[...].astype(BF16)
        b_copy(z, plane).start()
        return carry

    lax.fori_loop(1, n_q + 1, one_pass, 0)
    def finish_keys(whole):
        gk = collect(0, dk_sum, core_k_in, k_in, core_k, 0, first_in, whole)
        own_k[...] = gk

        @pl.when(low)
        def _():
            to(e_out.at[0], e_in.at[0], e_send.at[0], e_recv.at[0], partner).wait_recv()
            own_k[...] += e_in[0].astype(F32)

        gk = own_k[...] * scale
        gk_ref[...] = gk.astype(BF16)
        gkt[...] = gk.T.astype(BF16)

        def spread(chip):
            y_copy(chip).wait_recv()
            dw_out[chip] = (dw_out[chip].astype(F32) + x_in[chip].astype(F32)).astype(BF16)

            @pl.when(chip != u)
            def _():
                w_copy(chip, u).start()

        def project(i, carry):
            @pl.when(i < chips)
            def _():
                chip = lax.rem(u + 1 + i, chips)
                piece = nn(gkt[...], hid[:, pl.ds(pl.multiple_of(2 * width * chip, 2 * width), 2 * width)])
                left, right = piece[:, :width], piece[:, width:]
                dw_out[chip] = jnp.where(c == 0, left, right).astype(BF16)
                x_out[chip] = jnp.where(c == 0, right, left).astype(BF16)
                y_copy(chip).start()

            @pl.when(i >= LAG)
            def _():
                spread(lax.rem(u + 1 + i - LAG, chips))

            return carry

        lax.fori_loop(0, chips + LAG, project, 0)
        own_v[...] = collect(1, dv_sum, core_v_in, v_in, core_v, 0, first_in, whole)

        @pl.when(low)
        def _():
            to(e_out.at[1], e_in.at[1], e_send.at[1], e_recv.at[1], partner).wait_recv()
            own_v[...] += e_in[1].astype(F32)

        gv_ref[...] = own_v[...].astype(BF16)

    @pl.when(top)
    def _():
        finish_keys(False)

    @pl.when(jnp.logical_not(top))
    def _():
        finish_keys(True)

    def add_q(plane, carry):
        b_copy(plane, z).wait_recv()
        dq_own[...] += dq_in[plane].astype(F32)
        return carry

    @pl.when(z >= 2)
    def _():
        add_q(z - 1, 0)
        add_q(0, 0)

    for h in range(2 * heads):
        part = dq_own[h * HEAD_DIM:(h + 1) * HEAD_DIM, :]
        gq_ref[:, h * HEAD_DIM:(h + 1) * HEAD_DIM] = (part * scale).T.astype(BF16)

    def add_w(i, total):
        chip = chips - 1 - i
        w_copy(u, chip).wait_recv()
        return total + dw_in[chip].astype(F32)

    total = dw_out[u].astype(F32)
    total = lax.fori_loop(0, chips - 1 - u, add_w, total)
    total = lax.fori_loop(chips - u, chips, add_w, total)
    gw_ref[...] = total.T

    def kv_sent(base):
        for m, buf in ((0, kb), (1, vb)):
            f_copy(m, buf, base + y).wait_send()

        def sent(col):
            for m, buf in ((0, kb), (1, vb)):
                kv_copy(m, buf, base + y, col).wait_send()

        near(sent)

        def forwarded(col):
            for m, buf in ((0, kb), (1, vb)):
                f_copy(m, buf, base + col).wait_send()

        others(forwarded)
        if ring:
            for m, buf, step in ((0, kb, 3), (1, vb, 1)):
                g_copy(m, buf, 1 if base else 0, step).wait_send()

    kv_sent(0)

    @pl.when(odd)
    def _():
        kv_sent(ny)
        e_copy(0).wait_send()
        e_copy(1).wait_send()

    @pl.when(low)
    def _():
        h_copy(0, kb).wait_send()
        h_copy(1, vb).wait_send()

    @pl.when(z >= 2)
    def _():
        for m, buf in ((0, qn), (1, dn), (2, stats)):
            q_copy(m, buf, z, 0, q_send.at[m, 0]).wait_send()
        q_copy(2, stats, z, 0, q_send.at[2, 1]).wait_send()

    @pl.when(top)
    def _():
        q_copy(0, qn, z, 0, q_send.at[0, 1]).wait_send()
        q_copy(1, dn, z, 0, q_send.at[1, 1]).wait_send()

    @pl.when(z == 1)
    def _():
        q_copy(0, qn, z + 1, 0, r_send.at[0]).wait_send()
        q_copy(1, dn, z + 1, 0, r_send.at[1]).wait_send()

    def back_sent(p, carry):
        b_copy(z, jnp.where(z == 0, PLANES - p, z + 1)).wait_send()
        return carry

    lax.fori_loop(1, n_q + 1, back_sent, 0)

    def all_terms_sent(base, count, skipped):
        def terms_sent(col, carry):
            for m, src, dst in ((0, core_k, core_k_in), (1, core_v, core_v_in)):
                c_copy(m, src, dst, base + col).wait_send()

            @pl.when((col != y) & (col != skipped))
            def _():
                t_copy(0, k_out, k_in, base, y, col).wait_send()
                t_copy(1, v_out, v_in, base, y, col).wait_send()

            return carry

        lax.fori_loop(0, count, terms_sent, 0)

    def ring_sent(s):
        if ring:
            p_copy(0, k_out, s, 3).wait_send()
            p_copy(1, v_out, s, 1).wait_send()

    all_terms_sent(0, jnp.where(top, y + 1, ny), jnp.where(top, ny, turned(2)) if ring else ny)

    @pl.when(jnp.logical_not(top))
    def _():
        ring_sent(0)

    @pl.when(odd)
    def _():
        all_terms_sent(ny, ny, turned(2) if ring else ny)
        ring_sent(1)

    def dw_sent(chip, carry):
        y_copy(chip).wait_send()

        @pl.when(chip != u)
        def _():
            w_copy(chip, u).wait_send()

        return carry

    lax.fori_loop(0, chips, dw_sent, 0)


def on_device(n, hidden, key_weight, queries, values, map_out, log_sums, out_grad, mixing, out_gain):
    rows, model = hidden.shape
    heads = mixing.shape[0]
    k_cols = key_weight.shape[1]
    q_cols = queries.shape[1]
    chips = n // 2
    ny = chips // PLANES
    width = model // n
    vm = pltpu.VMEM
    dma = pltpu.SemaphoreType.DMA
    anywhere = pl.BlockSpec(memory_space=pl.ANY)
    inside = pl.BlockSpec(memory_space=pltpu.VMEM)
    tall = vm((2 * rows, heads * rows), BF16)
    slots = vm((2 * ny, rows, k_cols), BF16)
    results = pl.pallas_call(
        functools.partial(kernel, n, heads),
        out_shape=(
            jax.ShapeDtypeStruct((rows, q_cols), BF16),
            jax.ShapeDtypeStruct((rows, k_cols), BF16),
            jax.ShapeDtypeStruct((rows, V_DIM), BF16),
            jax.ShapeDtypeStruct((width, k_cols), F32),
        ),
        in_specs=[pl.BlockSpec(memory_space=pltpu.SMEM)] + [anywhere] * 8,
        out_specs=(inside,) * 4,
        scratch_shapes=[
            vm((rows, model), BF16),
            vm((model, k_cols), BF16),
            vm((rows, 2 * heads * V_DIM), BF16),
            vm((2 * heads, rows), F32),
            vm((rows, heads * V_DIM), BF16),
            vm((1, V_DIM), F32),
            vm((2 * ny, 2 * rows, k_cols), BF16),
            vm((2 * ny, 2 * rows, V_DIM), BF16),
            vm((2 * ny, k_cols, 2 * rows), BF16),
            vm((PLANES, rows, q_cols), BF16),
            vm((PLANES, rows, heads * V_DIM), BF16),
            vm((q_cols, rows), BF16),
            vm((heads * V_DIM, rows), BF16),
            vm((PLANES, 4 * heads, rows), F32),
            vm((q_cols, rows), F32),
            vm((q_cols, rows), F32),
            vm((PLANES, q_cols, rows), BF16),
            vm((PLANES, q_cols, rows), BF16),
            tall, tall, tall,
            vm((2 * ny, 2 * rows, k_cols), F32),
            vm((2 * ny, 2 * rows, V_DIM), F32),
            slots, slots, slots, slots, slots, slots, slots, slots,
            vm((k_cols, rows), BF16),
            vm((chips, k_cols, width), BF16),
            vm((chips, k_cols, width), BF16),
            vm((chips, k_cols, width), BF16),
            vm((chips, k_cols, width), BF16),
            vm((2, rows, k_cols), BF16),
            vm((2, rows, k_cols), BF16),
            vm((rows, k_cols), F32),
            vm((rows, V_DIM), F32),
            vm((2, 2, rows, k_cols), BF16),
            dma((8,)),
            dma((2, 2 * ny)), dma((2, 2 * ny)),
            dma((2, 2 * ny)), dma((2, 2 * ny)),
            dma((3, PLANES)), dma((3, PLANES)), dma((2,)),
            dma((PLANES,)), dma((PLANES,)),
            dma((2, 2 * ny)), dma((2, 2 * ny)),
            dma((2, 2 * ny)), dma((2, 2 * ny)),
            dma((chips,)), dma((chips,)),
            dma((chips,)), dma((chips,)),
            dma((2,)), dma((2,)),
            dma((2,)), dma((2,)),
            dma((2, 2)), dma((2, 2)),
            dma((2, 2)), dma((2, 2)),
        ],
        compiler_params=pltpu.CompilerParams(
            collective_id=0, has_side_effects=True, vmem_limit_bytes=63 * 1024 * 1024),
    )(mixing, hidden, key_weight, queries, values, map_out, log_sums, out_grad, out_gain.reshape(1, -1))
    return pl.pallas_call(
        write_out,
        out_shape=tuple(jax.ShapeDtypeStruct(r.shape, r.dtype) for r in results),
        in_specs=[inside] * 4,
        out_specs=(anywhere,) * 4,
        scratch_shapes=[dma((4,))],
    )(*results)


def solution(mesh):
    placed = (
        P("sp", None),
        P(None, "tp"),
        P("sp", "tp"),
        P("sp", "tp"),
        P("sp", "tp"),
        P("tp", "sp"),
        P("sp", "tp"),
        P("tp"),
        P(),
    )
    return jax.shard_map(
        functools.partial(on_device, mesh.shape["sp"]),
        mesh=mesh,
        in_specs=placed,
        out_specs=(P("sp", "tp"), P("sp", "tp"), P("sp", "tp"), P("sp", "tp")),
        check_vma=False,
    )
```

time: 107 us -> 101 us (0.944)
  local copies, waits for them, and re-layouts: 6.57 us -> 0 us
    unnamed x4 -> x0, local copies, waits for them, and re-layouts: 6.57 us -> none
    pallas_call x0 -> x1, Pallas kernels: none -> 2.12 us  [on_device(): pl.pallas_call(write_out, out_shape=tuple((jax.ShapeDtypeStruct(r.shape,...]
    pallas_call x1, Pallas kernels: 99.4 us -> 97.7 us  [on_device(): pl.pallas_call(functools.partial(kernel, n, heads), out_shape=(jax.ShapeD...]
where the time goes in v3:
time: 101 us
  Pallas kernels  99.9 us (99%)
    pallas_call x1, Pallas kernels, on_device(): pl.pallas_call(functools.partial(kernel, n, heads), out_shape=(jax.ShapeD...  97.7 us
    pallas_call x1, Pallas kernels, on_device(): pl.pallas_call(write_out, out_shape=tuple((jax.ShapeDtypeStruct(r.shape,...  2.12 us

profile of v3, /device:TPU:1, one launch (start us, length us, event | category | flops | bytes accessed | tf_op | source)
XLA Modules:
  0.0 100.7 jit_solution(1174276111050462495)
XLA Ops:
  0.6 97.7 %shard_map.120 = (bf16[256,1024]{1,0:T(8,128)(2,1)}, bf16[256,256]{1,0:T(8,128)(2,1)}, bf16[256,256]{1,0:T(8,128)(2,1)}, f32[128,256]{1,0:T(8,128)}) custom-call(f32[4]{0:T(128)} %mix_ref.1, bf16[256,4096]{1,0:T(8,128)(2,1)} %hid_hbm.1, bf16[4096,256]{1,0:T(8,128)(2,1)} %kw_hbm.1, bf16[256,1024]{1,0:T(8,128)(2,1)} %q_hbm.1, bf16[256,256]{1,0:T(8,128)(2,1)} %val_hbm.1, ...), custom_call_target="tpu_custom_call" | custom-call | tf_op jit(solution)/shard_map/pallas_call | solution.py:697
  98.4 2.1 %shard_map.121 = (bf16[256,1024]{1,0:T(8,128)(2,1)}, bf16[256,256]{1,0:T(8,128)(2,1)}, bf16[256,256]{1,0:T(8,128)(2,1)}, f32[128,256]{1,0:T(8,128)}) custom-call(bf16[256,1024]{1,0:T(8,128)(2,1)} %get-tuple-element.8.a, bf16[256,256]{1,0:T(8,128)(2,1)} %get-tuple-element.9.b, bf16[256,256]{1,0:T(8,128)(2,1)} %get-tuple-element.10.c, ...), custom_call_target="tpu_custom_call" | custom-call | tf_op jit(solution)/shard_map/pallas_call | solution.py:757

commit v4 on v3

--- a/solution.py
+++ b/solution.py
@@ -139,6 +139,15 @@
 
     def b_copy(source, dest):
         return to(dq_out.at[dest], dq_in.at[source], b_send.at[dest], b_recv.at[source], at(dest, y))
+
+    def back_copy(plane):
+        via = (z == 0) & (plane == PLANES - 2)
+        slot = jnp.where(via, 1, z)
+        return to(dq_out.at[plane], dq_in.at[slot], b_send.at[plane], b_recv.at[slot],
+                  at(jnp.where(via, PLANES - 1, plane), y))
+
+    def relay_copy():
+        return to(dq_in.at[1], dq_in.at[0], b_send.at[0], b_recv.at[0], at(PLANES - 2, y))
 
     def c_copy(m, src, dst, col):
         return to(src.at[col], dst.at[col], c_send.at[m, col], c_recv.at[m, col], partner)
@@ -501,7 +510,7 @@
 
         lax.fori_loop(1, ny + 1, one, 0)
         dq_out[plane] = dqt[...].astype(BF16)
-        b_copy(z, plane).start()
+        back_copy(plane).start()
         return carry
 
     lax.fori_loop(1, n_q + 1, one_pass, 0)
@@ -555,6 +564,8 @@
     @pl.when(top)
     def _():
         finish_keys(False)
+        b_copy(1, z).wait_recv()
+        relay_copy().start()
 
     @pl.when(jnp.logical_not(top))
     def _():
@@ -626,6 +637,7 @@
     def _():
         q_copy(0, qn, z, 0, q_send.at[0, 1]).wait_send()
         q_copy(1, dn, z, 0, q_send.at[1, 1]).wait_send()
+        relay_copy().wait_send()
 
     @pl.when(z == 1)
     def _():
@@ -633,7 +645,7 @@
         q_copy(1, dn, z + 1, 0, r_send.at[1]).wait_send()
 
     def back_sent(p, carry):
-        b_copy(z, jnp.where(z == 0, PLANES - p, z + 1)).wait_send()
+        back_copy(jnp.where(z == 0, PLANES - p, z + 1)).wait_send()
         return carry
 
     lax.fori_loop(1, n_q + 1, back_sent, 0)

time: 101 us -> 101 us (level)
  no operation moved by 1% of the time
where the time goes in v4:
time: 101 us
  Pallas kernels  99.9 us (99%)
    pallas_call x1, Pallas kernels, on_device(): pl.pallas_call(functools.partial(kernel, n, heads), out_shape=(jax.ShapeD...  97.7 us
    pallas_call x1, Pallas kernels, on_device(): pl.pallas_call(write_out, out_shape=tuple((jax.ShapeDtypeStruct(r.shape,...  2.12 us

profile of v4, /device:TPU:1, one launch (start us, length us, event | category | flops | bytes accessed | tf_op | source)
XLA Modules:
  0.0 100.7 jit_solution(11955589596407125919)
XLA Ops:
  0.6 97.7 %shard_map.120 = (bf16[256,1024]{1,0:T(8,128)(2,1)}, bf16[256,256]{1,0:T(8,128)(2,1)}, bf16[256,256]{1,0:T(8,128)(2,1)}, f32[128,256]{1,0:T(8,128)}) custom-call(f32[4]{0:T(128)} %mix_ref.1, bf16[256,4096]{1,0:T(8,128)(2,1)} %hid_hbm.1, bf16[4096,256]{1,0:T(8,128)(2,1)} %kw_hbm.1, bf16[256,1024]{1,0:T(8,128)(2,1)} %q_hbm.1, bf16[256,256]{1,0:T(8,128)(2,1)} %val_hbm.1, ...), custom_call_target="tpu_custom_call" | custom-call | tf_op jit(solution)/shard_map/pallas_call | solution.py:709
  98.4 2.1 %shard_map.121 = (bf16[256,1024]{1,0:T(8,128)(2,1)}, bf16[256,256]{1,0:T(8,128)(2,1)}, bf16[256,256]{1,0:T(8,128)(2,1)}, f32[128,256]{1,0:T(8,128)}) custom-call(bf16[256,1024]{1,0:T(8,128)(2,1)} %get-tuple-element.8.a, bf16[256,256]{1,0:T(8,128)(2,1)} %get-tuple-element.9.b, bf16[256,256]{1,0:T(8,128)(2,1)} %get-tuple-element.10.c, ...), custom_call_target="tpu_custom_call" | custom-call | tf_op jit(solution)/shard_map/pallas_call | solution.py:769
